TPU v7x, 32 devices: a whole 2x2x4 slice. The times are simulated.
32 devices in a mesh: sp: 8 (over z, y), tp: 4 (over x, core).
Axes of the slice: x: 2, y: 2, z: 4, core: 2. Of those that a mesh axis runs over, the one named last changes fastest.
Arguments:
- resid_in: bfloat16 [3072, 2048], P('sp'), may hold values from -6 to 6
- cotangent: bfloat16 [3072, 2048], P('sp'), may hold values from -2 to 2
- norm_gain: float32 [2048], replicated, may hold values from 0.1 to 1.9
- routes: int32 [3072, 2], P('sp'), may hold values from 0 to 7, all different within a row; in each aligned block of 384 rows (0 to 383, 384 to 767, ...) at most 192 rows name the same one
- route_weights: float32 [3072, 2], P('sp'), may hold values from 0.1 to 1
- gate_weight: bfloat16 [8, 2048, 1024], P('sp', None, 'tp'), may hold values from -0.125 to 0.125
- up_weight: bfloat16 [8, 2048, 1024], P('sp', None, 'tp'), may hold values from -0.125 to 0.125
- down_weight: bfloat16 [8, 1024, 2048], P('sp', 'tp'), may hold values from -0.1875 to 0.1875
- out_weight: bfloat16 [2048, 1024], P(None, 'tp'), may hold values from -0.1875 to 0.1875
- gate_b: bfloat16 [3072, 1024], P('sp', 'tp'), may hold values from -6 to 6
- gate_c: bfloat16 [3072, 1024], P('sp', 'tp'), may hold values from -6 to 6
- values_u: bfloat16 [3072, 1024], P('sp', 'tp'), may hold values from -6 to 6
- taps: float32 [3, 1024], P(None, 'tp'), may hold values from -3.5 to 3.5
Outputs:
- grad_gate_weight: float32 [8, 2048, 1024], P('sp', None, 'tp')
- grad_up_weight: float32 [8, 2048, 1024], P('sp', None, 'tp')
- grad_down_weight: float32 [8, 1024, 2048], P('sp', 'tp')
- grad_resid: bfloat16 [3072, 2048], P('sp')
- grad_out_weight: float32 [2048, 1024], P('sp', 'tp')
- grad_gate_b: bfloat16 [3072, 1024], P('sp', 'tp')
- grad_gate_c: bfloat16 [3072, 1024], P('sp', 'tp')
- grad_values: bfloat16 [3072, 1024], P('sp', 'tp')
Inputs may be any that keep to these rules, and one draw needn't show every extreme that they name: `routes`: A row's 2 experts differ. In the rows of one index of sp (384 tokens) no expert is named more than 192 times, a bound that some block reaches.
All inputs are finite; a program needn't handle non-finite values.
Results may differ from a plain program's by a relative error of at most 0.024.
Values may be sent and summed in bfloat16 or wider, within the bound.
A program may use at most 128 MiB of HBM per device.

v0:
```python
import jax
import jax.numpy as jnp
from jax import lax
from jax.sharding import PartitionSpec as P

norm_eps = 1e-06


def passed_along(array, axis, by):
    size = lax.axis_size(axis)
    pairs = [(i, i + by) for i in range(size) if 0 <= i + by < size]
    return lax.ppermute(array, axis, pairs)


def expert_pass(entry_rows, entry_cots, entry_weights, gate_mat, up_mat, down_mat):
    f32 = jnp.float32
    bf16 = jnp.bfloat16
    gate_pre = jnp.dot(entry_rows, gate_mat, preferred_element_type=f32)
    up_pre = jnp.dot(entry_rows, up_mat, preferred_element_type=f32)
    logistic = jax.nn.sigmoid(gate_pre)
    activated = gate_pre * logistic
    hidden = (activated * up_pre * entry_weights[:, None]).astype(bf16)
    grad_down = jnp.einsum("rf,rd->fd", hidden, entry_cots, preferred_element_type=f32)
    dhidden = (
        jnp.einsum("rd,fd->rf", entry_cots, down_mat, preferred_element_type=f32)
        * entry_weights[:, None]
    )
    dgate = (dhidden * up_pre * logistic * (1.0 + gate_pre * (1.0 - logistic))).astype(bf16)
    dup = (dhidden * activated).astype(bf16)
    grad_gate = jnp.einsum("rd,rf->df", entry_rows, dgate, preferred_element_type=f32)
    grad_up = jnp.einsum("rd,rf->df", entry_rows, dup, preferred_element_type=f32)
    partial_sum = jnp.einsum("rf,df->rd", dgate, gate_mat, preferred_element_type=f32) + jnp.einsum(
        "rf,df->rd", dup, up_mat, preferred_element_type=f32
    )
    return (grad_gate, grad_up, grad_down, partial_sum)


def on_device(
    resid_in,
    cotangent,
    norm_gain,
    routes,
    route_weights,
    gate_weight,
    up_weight,
    down_weight,
    out_weight,
    gate_b,
    gate_c,
    values_u,
    taps,
):
    f32 = jnp.float32
    bf16 = jnp.bfloat16
    token_count, model_width = resid_in.shape
    groups = lax.axis_size("sp")
    lanes = lax.axis_size("tp")
    local_experts = gate_weight.shape[0]
    expert_total = local_experts * groups
    capacity = 4 * token_count // expert_total
    slot_span = local_experts * capacity
    resid_wide = resid_in.astype(f32)
    inv_rms = lax.rsqrt(jnp.mean(resid_wide * resid_wide, axis=1, keepdims=True) + norm_eps)
    normed = (resid_wide * inv_rms * norm_gain).astype(bf16)
    mixed = gate_c.astype(f32) * values_u.astype(f32)
    earlier = passed_along(mixed[-2:], "sp", 1)
    flat_routes = routes.reshape(-1)
    one_hot = (flat_routes[:, None] == jnp.arange(expert_total, dtype=jnp.int32)[None, :]).astype(
        jnp.int32
    )
    before = jnp.cumsum(one_hot, axis=0) - one_hot
    slot_rank = jnp.sum(before * one_hot, axis=1)
    targets = flat_routes * capacity + slot_rank
    sent_rows = (
        jnp.zeros((expert_total * capacity, model_width), bf16)
        .at[targets]
        .set(jnp.repeat(normed, 2, axis=0))
        .reshape(groups, slot_span, model_width)
    )
    sent_cots = (
        jnp.zeros((expert_total * capacity, model_width), bf16)
        .at[targets]
        .set(jnp.repeat(cotangent, 2, axis=0))
        .reshape(groups, slot_span, model_width)
    )
    sent_weights = (
        jnp.zeros((expert_total * capacity,), f32)
        .at[targets]
        .set(route_weights.reshape(-1))
        .reshape(groups, slot_span)
    )
    got_rows, got_cots, got_weights = (
        lax.all_to_all(sent_rows, "sp", split_axis=0, concat_axis=0, tiled=True),
        lax.all_to_all(sent_cots, "sp", split_axis=0, concat_axis=0, tiled=True),
        lax.all_to_all(
            sent_weights.astype(jnp.bfloat16), "sp", split_axis=0, concat_axis=0, tiled=True
        ).astype(sent_weights.dtype),
    )
    grads_gate, grads_up, grads_down, terms = ([], [], [], [])
    entry_rows = got_rows.reshape(groups * capacity, model_width)
    entry_cots = got_cots.reshape(groups * capacity, model_width)
    entry_weights = got_weights.reshape(groups * capacity)
    grad_gate, grad_up, grad_down, partial_sum = expert_pass(
        entry_rows, entry_cots, entry_weights, gate_weight[0], up_weight[0], down_weight[0]
    )
    grads_gate.append(grad_gate)
    grads_up.append(grad_up)
    grads_down.append(grad_down)
    terms.append(partial_sum.astype(bf16).reshape(groups, capacity, model_width))
    expert_term = terms[0]
    summed = (
        lax.psum_scatter(expert_term, "tp", scatter_dimension=2, tiled=True)
        .astype(jnp.float32)
        .astype(bf16)
    )
    returned = lax.all_to_all(summed, "sp", split_axis=0, concat_axis=0, tiled=True).reshape(
        expert_total * capacity, model_width // lanes
    )
    slot_grads = returned[targets].astype(f32).reshape(token_count, 2, model_width // lanes)
    dnormed = lax.all_gather(
        (slot_grads[:, 0] + slot_grads[:, 1]).astype(jnp.bfloat16), "tp", axis=1, tiled=True
    ).astype(jnp.float32)
    scaled = dnormed * norm_gain
    resid_grad = (
        cotangent.astype(f32)
        + inv_rms * scaled
        - resid_wide * inv_rms**3 * jnp.mean(scaled * resid_wide, axis=1, keepdims=True)
    )
    grad_resid = resid_grad.astype(bf16)
    extended = jnp.concatenate([earlier, mixed], axis=0)
    conv = (
        taps[0] * extended[:token_count]
        + taps[1] * extended[1 : token_count + 1]
        + taps[2] * extended[2 : token_count + 2]
    )
    merged = (gate_b.astype(f32) * conv).astype(bf16)
    grad_out_weight = lax.psum_scatter(
        jnp.einsum("td,tc->dc", grad_resid, merged, preferred_element_type=f32).astype(
            jnp.bfloat16
        ),
        "sp",
        scatter_dimension=0,
        tiled=True,
    ).astype(jnp.float32)
    dmerged = jnp.dot(grad_resid, out_weight, preferred_element_type=f32)
    grad_gate_b = (dmerged * conv).astype(bf16)
    dconv = dmerged * gate_b.astype(f32)
    later = passed_along(dconv[:2], "sp", -1)
    extended_grad = jnp.concatenate([dconv, later], axis=0)
    dmixed = (
        taps[2] * extended_grad[:token_count]
        + taps[1] * extended_grad[1 : token_count + 1]
        + taps[0] * extended_grad[2 : token_count + 2]
    )
    grad_gate_c = (dmixed * values_u.astype(f32)).astype(bf16)
    grad_values = (dmixed * gate_c.astype(f32)).astype(bf16)
    return (
        jnp.stack(grads_gate),
        jnp.stack(grads_up),
        jnp.stack(grads_down),
        grad_resid,
        grad_out_weight,
        grad_gate_b,
        grad_gate_c,
        grad_values,
    )


def solution(mesh):
    placed = (
        P("sp", None),
        P("sp", None),
        P(),
        P("sp", None),
        P("sp", None),
        P("sp", None, "tp"),
        P("sp", None, "tp"),
        P("sp", "tp", None),
        P(None, "tp"),
        P("sp", "tp"),
        P("sp", "tp"),
        P("sp", "tp"),
        P(None, "tp"),
    )
    return jax.shard_map(
        on_device,
        mesh=mesh,
        in_specs=placed,
        out_specs=(
            P("sp", None, "tp"),
            P("sp", None, "tp"),
            P("sp", "tp", None),
            P("sp", None),
            P("sp", "tp"),
            P("sp", "tp"),
            P("sp", "tp"),
            P("sp", "tp"),
        ),
        check_vma=False,
    )
```

profile of v0, /device:TPU:0, one launch (start us, length us, event | category | flops | bytes accessed | tf_op | source)
XLA Modules:
  0.0 555.7 jit_solution(14058691424197702794)
XLA Ops:
  12.7 3.4 scatter_custom_fusion.2
  16.8 7.3 %all-to-all-start.2 = ((bf16[8,1,192]{2,1,0:T(2,128)(2,1)}), bf16[8,1,192]{2,1,0:T(2,128)(2,1)S(1)}, u32[]{:S(2)}, u32[]{:S(2)}) async-start(bf16[8,1,192]{2,1,0:T(2,128)(2,1)} %convert_element_type.133), calls=%async_computation.2 | async-start | bytes 16384 | tf_op jit(solution)/shard_map/all_to_all | solution.py:95
  27.5 5.0 broadcast_in_dim.6
  32.5 5.7 %reshape.159 = bf16[768,2048]{1,0:T(8,128)(2,1)} reshape(bf16[384,2,2048]{2,1,0:T(2,128)(2,1)} %broadcast_in_dim.6) | data formatting | bytes 6291456 | tf_op jit(solution)/shard_map/reshape | solution.py:77
  38.2 11.6 %scatter_custom_fusion = bf16[1536,2048]{1,0:T(8,128)(2,1)} fusion(s32[768]{0:T(1024)S(1)} %fusion.44, bf16[768,2048]{1,0:T(8,128)(2,1)} %reshape.159, bf16[]{:T(256)} %constant.8.clone.1), kind=kCustom, calls=%fused_computation.21 | custom fusion | bytes 6291968 | tf_op jit(solution)/shard_map/scatter | solution.py:77
  49.8 6.4 %all-to-all-start = ((bf16[8,192,2048]{2,1,0:T(8,128)(2,1)}), bf16[8,192,2048]{2,1,0:T(8,128)(2,1)}, u32[]{:S(2)}, u32[]{:S(2)}) async-start(bf16[8,192,2048]{2,1,0:T(8,128)(2,1)} %bitcast.59), calls=%async_computation | async-start | bytes 12582912 | tf_op jit(solution)/shard_map/all_to_all | solution.py:93
  56.2 3.5 broadcast_in_dim.7
  59.8 5.7 %reshape.167 = bf16[768,2048]{1,0:T(8,128)(2,1)} reshape(bf16[384,2,2048]{2,1,0:T(2,128)(2,1)} %broadcast_in_dim.7) | data formatting | bytes 6291456 | tf_op jit(solution)/shard_map/reshape | solution.py:83
  65.5 11.5 %scatter_custom_fusion.1 = bf16[1536,2048]{1,0:T(8,128)(2,1)} fusion(s32[768]{0:T(1024)S(1)} %fusion.44, bf16[768,2048]{1,0:T(8,128)(2,1)} %reshape.167, bf16[]{:T(256)} %constant.8.clone.1), kind=kCustom, calls=%fused_computation.19 | custom fusion | bytes 6291968 | tf_op jit(solution)/shard_map/scatter | solution.py:83
  77.0 116.8 %all-to-all-done = bf16[8,192,2048]{2,1,0:T(8,128)(2,1)} async-done(((bf16[8,192,2048]{2,1,0:T(8,128)(2,1)}), bf16[8,192,2048]{2,1,0:T(8,128)(2,1)}, u32[]{:S(2)}, u32[]{:S(2)}) %all-to-all-start) | async-done | bytes 6291488 | tf_op jit(solution)/shard_map/all_to_all | solution.py:93
  193.8 4.8 all-to-all-start.1
  198.9 5.8 %fusion.16 = f32[1536,256]{1,0:T(8,128)} fusion(bf16[1536,2048]{1,0:T(8,128)(2,1)} %bitcast.4, bf16[1,2048,256]{2,1,0:T(8,128)(2,1)S(1)} %copy-done), kind=kOutput, calls=%fused_computation.35 | convolution fusion | flops 1610612736 | bytes 8912896 | tf_op jit(solution)/shard_map/dot_general | solution.py:18
  204.8 5.7 %fusion.19 = f32[1536,256]{1,0:T(8,128)} fusion(bf16[1536,2048]{1,0:T(8,128)(2,1)} %bitcast.4, bf16[1,2048,256]{2,1,0:T(8,128)(2,1)S(1)} %copy-done.7), kind=kOutput, calls=%fused_computation.38 | convolution fusion | flops 1610612736 | bytes 8912896 | tf_op jit(solution)/shard_map/dot_general | solution.py:19
  210.5 125.4 %all-to-all-done.1 = bf16[8,192,2048]{2,1,0:T(8,128)(2,1)} async-done(((bf16[8,192,2048]{2,1,0:T(8,128)(2,1)}), bf16[8,192,2048]{2,1,0:T(8,128)(2,1)}, u32[]{:S(2)}, u32[]{:S(2)}) %all-to-all-start.1) | async-done | bytes 6291488 | tf_op jit(solution)/shard_map/all_to_all | solution.py:94
  335.9 6.4 %multiply_convert_fusion.1 = (bf16[1536,256]{1,0:T(8,128)(2,1)S(1)}, bf16[1536,256]{1,0:T(8,128)(2,1)S(1)}) fusion(f32[1536,256]{1,0:T(8,128)} %fusion.16, f32[1536,256]{1,0:T(8,128)} %fusion.19, f32[1536]{0:T(1024)S(1)} %reshape.145, bf16[1536,2048]{1,0:T(8,128)(2,1)} %bitcast.6, bf16[1,256,2048]{2,1,0:T(8,128)(2,1)} %param.20), kind=kOutput, calls=%fused_computation.29 | convolution fusion | flops 1616117760 | bytes 12064768 | tf_op jit(solution)/shard_map/rd,fd->rf/dot_general | solution.py:25
  342.2 1.8 fusion.14
  344.1 4.4 add_convert_fusion
  348.5 57.1 %reduce-scatter.3.cloned.1.call-done = bf16[8,192,512]{2,1,0:T(8,128)(2,1)} async-done(((bf16[8,192,2048]{2,1,0:T(8,128)(2,1)}), bf16[8,192,512]{2,1,0:T(8,128)(2,1)}) %reduce-scatter.3.cloned.1.call-update) | async-done | bytes 1572880 | tf_op jit(solution)/shard_map/reduce_scatter | solution.py:112
  405.6 5.5 all-to-all-start.3
  411.4 36.5 %all-to-all-done.3 = bf16[8,192,512]{2,1,0:T(8,128)(2,1)S(1)} async-done(((bf16[8,192,512]{2,1,0:T(8,128)(2,1)}), bf16[8,192,512]{2,1,0:T(8,128)(2,1)S(1)}, u32[]{:S(2)}, u32[]{:S(2)}) %all-to-all-start.3) | async-done | bytes 1572896 | tf_op jit(solution)/shard_map/all_to_all | solution.py:116
  448.0 2.7 gather_fusion
  450.7 2.1 reshape.146
  452.8 3.4 fusion.48
  458.1 3.3 collective-permute-start
  461.4 13.5 %all-gather.3.cloned.1.call-done = bf16[384,1,2048]{2,0,1:T(8,128)(2,1)} async-done(((bf16[384,1,512]{2,0,1:T(8,128)(2,1)}), bf16[384,1,2048]{2,0,1:T(8,128)(2,1)}) %all-gather.3.cloned.1.call-update) | async-done | bytes 1572880 | tf_op jit(solution)/shard_map/all_gather | solution.py:120
  474.9 2.1 fusion.6
  477.1 2.5 fusion.5
  480.9 1.8 convolution_convert_fusion
  482.8 6.2 %convolution_bitcast_fusion.2 = f32[1,2048,256]{2,1,0:T(8,128)} fusion(bf16[1536,2048]{1,0:T(8,128)(2,1)} %bitcast.4, bf16[1536,256]{1,0:T(8,128)(2,1)S(1)} %get-tuple-element.13), kind=kOutput, calls=%fused_computation.26 | convolution fusion | flops 1610612736 | bytes 9175040 | tf_op jit(solution)/shard_map/rd,rf->df/dot_general | solution.py:30
  489.0 6.3 %convolution_bitcast_fusion = f32[1,256,2048]{2,1,0:T(8,128)} fusion(bf16[1536,2048]{1,0:T(8,128)(2,1)} %bitcast.6, f32[1536,256]{1,0:T(8,128)S(1)} %copy-done.18, f32[1536]{0:T(1024)S(1)} %reshape.145, f32[1536,256]{1,0:T(8,128)S(1)} %copy-done.17), kind=kOutput, calls=%fused_computation.24 | convolution fusion | flops 1613365248 | bytes 11540480 | tf_op jit(solution)/shard_map/rf,rd->fd/dot_general | solution.py:23
  496.7 6.1 %convolution_bitcast_fusion.1 = f32[1,2048,256]{2,1,0:T(8,128)} fusion(bf16[1536,2048]{1,0:T(8,128)(2,1)} %bitcast.4, bf16[1536,256]{1,0:T(8,128)(2,1)S(1)} %copy-done.9), kind=kOutput, calls=%fused_computation.25 | convolution fusion | flops 1610612736 | bytes 9175040 | tf_op jit(solution)/shard_map/rd,rf->df/dot_general | solution.py:31
  504.4 42.7 %reduce-scatter.5.cloned.1.call-done = bf16[256,256]{1,0:T(8,128)(2,1)} async-done(((bf16[2048,256]{1,0:T(8,128)(2,1)}), bf16[256,256]{1,0:T(8,128)(2,1)}) %reduce-scatter.5.cloned.1.call-update) | async-done | bytes 131088 | tf_op jit(solution)/shard_map/reduce_scatter | solution.py:137
  (82 shorter events, 18.1 us)
Async XLA Ops:
  7.2 191.8 %copy-start = (bf16[1,2048,256]{2,1,0:T(8,128)(2,1)S(1)}, bf16[1,2048,256]{2,1,0:T(8,128)(2,1)}, u32[]{:S(2)}) copy-start(bf16[1,2048,256]{2,1,0:T(8,128)(2,1)} %param.18) | copy-start | bytes 3145732
  7.2 18.8 %copy-start.2 = (bf16[384,2048]{1,0:T(8,128)(2,1)S(1)}, bf16[384,2048]{1,0:T(8,128)(2,1)}, u32[]{:S(2)}) copy-start(bf16[384,2048]{1,0:T(8,128)(2,1)} %param.13) | copy-start | bytes 4718596
  7.2 18.8 %copy-start.13 = (f32[2048]{0:T(1024)S(1)}, f32[2048]{0:T(1024)}, u32[]{:S(2)}) copy-start(f32[2048]{0:T(1024)} %param.15) | copy-start | bytes 24580
  16.8 33.0 %all-to-all-start.2 = ((bf16[8,1,192]{2,1,0:T(2,128)(2,1)}), bf16[8,1,192]{2,1,0:T(2,128)(2,1)S(1)}, u32[]{:S(2)}, u32[]{:S(2)}) async-start(bf16[8,1,192]{2,1,0:T(2,128)(2,1)} %convert_element_type.133), calls=%async_computation.2 | async-start | bytes 16384 | tf_op jit(solution)/shard_map/all_to_all | solution.py:95
  49.8 6.4 %copy-start.4 = (bf16[384,2048]{1,0:T(8,128)(2,1)S(1)}, bf16[384,2048]{1,0:T(8,128)(2,1)}, u32[]{:S(2)}) copy-start(bf16[384,2048]{1,0:T(8,128)(2,1)} %param.14) | copy-start | bytes 4718596
  49.8 144.0 %all-to-all-start = ((bf16[8,192,2048]{2,1,0:T(8,128)(2,1)}), bf16[8,192,2048]{2,1,0:T(8,128)(2,1)}, u32[]{:S(2)}, u32[]{:S(2)}) async-start(bf16[8,192,2048]{2,1,0:T(8,128)(2,1)} %bitcast.59), calls=%async_computation | async-start | bytes 12582912 | tf_op jit(solution)/shard_map/all_to_all | solution.py:93
  193.8 142.1 %all-to-all-start.1 = ((bf16[8,192,2048]{2,1,0:T(8,128)(2,1)}), bf16[8,192,2048]{2,1,0:T(8,128)(2,1)}, u32[]{:S(2)}, u32[]{:S(2)}) async-start(bf16[8,192,2048]{2,1,0:T(8,128)(2,1)} %bitcast.58), calls=%async_computation.1 | async-start | bytes 12582912 | tf_op jit(solution)/shard_map/all_to_all | solution.py:94
  198.6 207.1 %reduce-scatter.3.cloned.1.call-start = ((), (), s32[]{:S(2)}) async-start(), calls=%async_computation.6 | async-start | bytes 7864320 | tf_op jit(solution)/shard_map/reduce_scatter | solution.py:112
  198.9 5.8 %copy-start.7 = (bf16[1,2048,256]{2,1,0:T(8,128)(2,1)S(1)}, bf16[1,2048,256]{2,1,0:T(8,128)(2,1)}, u32[]{:S(2)}) copy-start(bf16[1,2048,256]{2,1,0:T(8,128)(2,1)} %param.19) | copy-start | bytes 3145732
  342.2 1.8 copy-start.8
  405.6 42.3 %all-to-all-start.3 = ((bf16[8,192,512]{2,1,0:T(8,128)(2,1)}), bf16[8,192,512]{2,1,0:T(8,128)(2,1)S(1)}, u32[]{:S(2)}, u32[]{:S(2)}) async-start(bf16[8,192,512]{2,1,0:T(8,128)(2,1)} %reduce-scatter.3.cloned.1.call-done), calls=%async_computation.4 | async-start | bytes 3145728 | tf_op jit(solution)/shard_map/all_to_all | solution.py:116
  411.1 63.8 %all-gather.3.cloned.1.call-start = ((), (), s32[]{:S(2)}) async-start(), calls=%async_computation.8 | async-start | bytes 1966080 | tf_op jit(solution)/shard_map/all_gather | solution.py:120
  452.8 4.3 copy-start.10
  452.8 8.6 %copy-start.14 = (f32[3,256]{1,0:T(4,128)S(1)}, f32[3,256]{1,0:T(4,128)}, u32[]{:S(2)}) copy-start(f32[3,256]{1,0:T(4,128)} %param.25) | copy-start | bytes 9220
  452.8 22.2 %copy-start.3 = (bf16[384,2048]{1,0:T(8,128)(2,1)S(1)}, bf16[384,2048]{1,0:T(8,128)(2,1)}, u32[]{:S(2)}) copy-start(bf16[384,2048]{1,0:T(8,128)(2,1)} %param.13) | copy-start | bytes 4718596
  457.0 90.1 %reduce-scatter.5.cloned.1.call-start = ((), (), s32[]{:S(2)}) async-start(), calls=%async_computation.7 | async-start | bytes 1179648 | tf_op jit(solution)/shard_map/reduce_scatter | solution.py:137
  458.1 21.6 %collective-permute-start = (f32[2,256]{1,0:T(2,128)S(1)}, f32[2,256]{1,0:T(2,128)S(1)}, u32[]{:S(2)}, u32[]{:S(2)}) collective-permute-start(f32[2,256]{1,0:T(2,128)S(1)} %slice.60), channel_id=1, source_target_pairs={{0,4},{4,8},{8,12},{12,16},{16,20},{20,24},{24,28},{1,5},{5,9},{9,... | collective-permute-start | bytes 6152 | tf_op jit(solution)/shard_map/ppermute | solution.py:12
  474.9 2.1 copy-start.5
  477.1 2.6 copy-start.15
  477.1 2.6 copy-start.16
  479.6 1.3 copy-start.6
  482.8 6.2 %copy-start.17 = (f32[1536,256]{1,0:T(8,128)S(1)}, f32[1536,256]{1,0:T(8,128)}, u32[]{:S(2)}) copy-start(f32[1536,256]{1,0:T(8,128)} %fusion.16) | copy-start | bytes 4718596
  482.8 6.2 %copy-start.18 = (f32[1536,256]{1,0:T(8,128)S(1)}, f32[1536,256]{1,0:T(8,128)}, u32[]{:S(2)}) copy-start(f32[1536,256]{1,0:T(8,128)} %fusion.19) | copy-start | bytes 4718596
  489.0 7.7 %copy-start.9 = (bf16[1536,256]{1,0:T(8,128)(2,1)S(1)}, bf16[1536,256]{1,0:T(8,128)(2,1)}, u32[]{:S(2)}) copy-start(bf16[1536,256]{1,0:T(8,128)(2,1)} %copy-done.8) | copy-start | bytes 2359300
  495.3 7.6 %copy-start.12 = (bf16[384,256]{1,0:T(8,128)(2,1)S(1)}, bf16[384,256]{1,0:T(8,128)(2,1)}, u32[]{:S(2)}) copy-start(bf16[384,256]{1,0:T(8,128)(2,1)} %param.23) | copy-start | bytes 589828
  495.3 8.4 %copy-start.11 = (bf16[384,256]{1,0:T(8,128)(2,1)S(1)}, bf16[384,256]{1,0:T(8,128)(2,1)}, u32[]{:S(2)}) copy-start(bf16[384,256]{1,0:T(8,128)(2,1)} %param.24) | copy-start | bytes 589828
  495.3 7.6 %collective-permute-start.1 = (f32[2,256]{1,0:T(2,128)S(1)}, f32[2,256]{1,0:T(2,128)S(1)}, u32[]{:S(2)}, u32[]{:S(2)}) collective-permute-start(f32[2,256]{1,0:T(2,128)S(1)} %slice.63), channel_id=1, source_target_pairs={{4,0},{8,4},{12,8},{16,12},{20,16},{24,20},{28,24},{5,1},{9,5},{13... | collective-permute-start | bytes 6152 | tf_op jit(solution)/shard_map/ppermute | solution.py:12
  496.7 52.1 %copy-start.1 = (bf16[1,2048,256]{2,1,0:T(8,128)(2,1)S(1)}, bf16[1,2048,256]{2,1,0:T(8,128)(2,1)}, u32[]{:S(2)}) copy-start(bf16[1,2048,256]{2,1,0:T(8,128)(2,1)} %param.18) | copy-start | bytes 3145732
Sparse Core Ops, SparseCore 0:
  348.7 56.9 reduce-scatter.2
  457.1 17.7 all-gather.2
  482.9 64.1 reduce-scatter.4
where the time goes:
time: 565 us; the launch traced here: 556 us
  waiting for transfers between devices  392 us (69%)
  local copies, waits for them, and re-layouts  58.2 us (10%)
  matrix products  45.8 us (8%)
  starting transfers between devices  29.2 us (5%)
  other arithmetic  15.9 us (3%)
  between operations  14.5 us (3%)
    all_to_all x1, waiting for transfers between devices, on_device(): lax.all_to_all(sent_cots, 'sp', split_axis=0, concat_axis=0, tiled=True)  125 us
    all_to_all x1, waiting for transfers between devices, on_device(): lax.all_to_all(sent_rows, 'sp', split_axis=0, concat_axis=0, tiled=True)  117 us
    reduce_scatter x1, waiting for transfers between devices, on_device(): lax.psum_scatter(expert_term, 'tp', scatter_dimension=2, tiled=True)  57.1 us
    reduce_scatter x1, waiting for transfers between devices, on_device(): lax.psum_scatter(jnp.einsum('td,tc->dc', grad_resid, merged, preferred_el...  42.7 us
    all_to_all x1, waiting for transfers between devices, on_device(): lax.all_to_all(summed, 'sp', split_axis=0, concat_axis=0, tiled=True)  36.5 us
    all_gather x1, waiting for transfers between devices, on_device(): lax.all_gather((slot_grads[:, 0] + slot_grads[:, 1]).astype(jnp.bfloat16)...  13.5 us
    scatter x1, local copies, waits for them, and re-layouts, on_device(): sent_rows = jnp.zeros((expert_total * capacity, model_width), bf16).at[ta...  11.6 us
    scatter x1, local copies, waits for them, and re-layouts, on_device(): sent_cots = jnp.zeros((expert_total * capacity, model_width), bf16).at[ta...  11.5 us
  transfers between devices with their start and end apart: 9, of which 6 were waited for; matrix products, arithmetic and copies ran while one was open for 15% of the time, Pallas kernels for 0%

commit v1 on v0

--- a/solution.py
+++ b/solution.py
@@ -64,37 +64,40 @@
     normed = (resid_wide * inv_rms * norm_gain).astype(bf16)
     mixed = gate_c.astype(f32) * values_u.astype(f32)
     earlier = passed_along(mixed[-2:], "sp", 1)
-    flat_routes = routes.reshape(-1)
-    one_hot = (flat_routes[:, None] == jnp.arange(expert_total, dtype=jnp.int32)[None, :]).astype(
-        jnp.int32
-    )
-    before = jnp.cumsum(one_hot, axis=0) - one_hot
-    slot_rank = jnp.sum(before * one_hot, axis=1)
-    targets = flat_routes * capacity + slot_rank
-    sent_rows = (
-        jnp.zeros((expert_total * capacity, model_width), bf16)
-        .at[targets]
-        .set(jnp.repeat(normed, 2, axis=0))
-        .reshape(groups, slot_span, model_width)
-    )
-    sent_cots = (
-        jnp.zeros((expert_total * capacity, model_width), bf16)
-        .at[targets]
-        .set(jnp.repeat(cotangent, 2, axis=0))
-        .reshape(groups, slot_span, model_width)
-    )
-    sent_weights = (
-        jnp.zeros((expert_total * capacity,), f32)
-        .at[targets]
-        .set(route_weights.reshape(-1))
-        .reshape(groups, slot_span)
-    )
-    got_rows, got_cots, got_weights = (
+    quarter = model_width // lanes
+    lane = lax.axis_index("tp")
+    slots = expert_total * capacity
+    names = jnp.arange(expert_total, dtype=jnp.int32)
+    chosen = routes[:, :, None] == names[None, None, :]
+    named = jnp.any(chosen, axis=1).astype(bf16)
+    order = jnp.arange(token_count, dtype=jnp.int32)
+    strict = (order[:, None] > order[None, :]).astype(bf16)
+    before = jnp.dot(strict, named, preferred_element_type=f32).astype(jnp.int32)
+    rank = jnp.sum(jnp.where(chosen, before[:, None, :], 0), axis=2)
+    targets = routes * capacity + rank
+    slot_ids = jnp.arange(slots, dtype=jnp.int32)[:, None]
+    first = slot_ids == targets[:, 0][None, :]
+    second = slot_ids == targets[:, 1][None, :]
+    placing = (first | second).astype(bf16)
+    sent_weights = jnp.sum(
+        jnp.where(first, route_weights[:, 0][None, :], 0.0)
+        + jnp.where(second, route_weights[:, 1][None, :], 0.0),
+        axis=1,
+    ).reshape(groups, slot_span)
+    own_rows = lax.dynamic_slice_in_dim(normed, lane * quarter, quarter, axis=1)
+    own_cots = lax.dynamic_slice_in_dim(cotangent, lane * quarter, quarter, axis=1)
+    sent_rows = jnp.dot(placing, own_rows, preferred_element_type=f32).astype(bf16)
+    sent_cots = jnp.dot(placing, own_cots, preferred_element_type=f32).astype(bf16)
+    sent_rows = sent_rows.reshape(groups, slot_span, quarter)
+    sent_cots = sent_cots.reshape(groups, slot_span, quarter)
+    got_weights = lax.all_to_all(sent_weights, "sp", split_axis=0, concat_axis=0, tiled=True)
+    got_rows = lax.all_gather(
         lax.all_to_all(sent_rows, "sp", split_axis=0, concat_axis=0, tiled=True),
+        "tp", axis=2, tiled=True,
+    )
+    got_cots = lax.all_gather(
         lax.all_to_all(sent_cots, "sp", split_axis=0, concat_axis=0, tiled=True),
-        lax.all_to_all(
-            sent_weights.astype(jnp.bfloat16), "sp", split_axis=0, concat_axis=0, tiled=True
-        ).astype(sent_weights.dtype),
+        "tp", axis=2, tiled=True,
     )
     grads_gate, grads_up, grads_down, terms = ([], [], [], [])
     entry_rows = got_rows.reshape(groups * capacity, model_width)
@@ -116,10 +119,8 @@
     returned = lax.all_to_all(summed, "sp", split_axis=0, concat_axis=0, tiled=True).reshape(
         expert_total * capacity, model_width // lanes
     )
-    slot_grads = returned[targets].astype(f32).reshape(token_count, 2, model_width // lanes)
-    dnormed = lax.all_gather(
-        (slot_grads[:, 0] + slot_grads[:, 1]).astype(jnp.bfloat16), "tp", axis=1, tiled=True
-    ).astype(jnp.float32)
+    own_grad = jnp.einsum("st,sq->tq", placing, returned, preferred_element_type=f32)
+    dnormed = lax.all_gather(own_grad.astype(bf16), "tp", axis=1, tiled=True).astype(f32)
     scaled = dnormed * norm_gain
     resid_grad = (
         cotangent.astype(f32)

time: 565 us -> 365 us (0.65); the launches traced: 556 us -> 364 us
  waiting for transfers between devices: 392 us -> 145 us
  blocking collectives: 0 us -> 137 us
  local copies, waits for them, and re-layouts: 58.2 us -> 0.9 us
  starting transfers between devices: 29.2 us -> 5.21 us
    all_to_all x4 -> x0, waiting for transfers between devices: 279 us -> none  [the longest x1 125 us: on_device(): lax.all_to_all(sent_cots, 'sp', split_axis=0, concat_axis=0, tiled=True)]
    all_to_all x0 -> x4, blocking collectives: none -> 137 us  [the longest x1 44.2 us: on_device(): lax.all_to_all(sent_rows, 'sp', split_axis=0, concat_axis=0, tiled=True)]
    all_gather x1 -> x3, waiting for transfers between devices: 13.5 us -> 44.4 us  [the longest x1 30.3 us: on_device(): lax.all_gather(lax.all_to_all(sent_cots, 'sp', split_axis=0, concat_axis=...]
    scatter x3 -> x0, local copies, waits for them, and re-layouts: 26.5 us -> none  [the longest x1 11.6 us: on_device(): sent_rows = jnp.zeros((expert_total * capacity, model_width), bf16).at[ta...]
    all_to_all x4 -> x0, starting transfers between devices: 23.9 us -> none  [the longest x1 7.31 us: on_device(): lax.all_to_all(sent_weights.astype(jnp.bfloat16), 'sp', split_axis=0, con...]
    reshape x3 -> x0, local copies, waits for them, and re-layouts: 11.6 us -> none  [the longest x1 5.73 us: on_device(): jnp.repeat(cotangent, 2, axis=0)]
    broadcast_in_dim x2 -> x0, local copies, waits for them, and re-layouts: 8.54 us -> none  [the longest x1 4.99 us: on_device(): jnp.repeat(normed, 2, axis=0)]
    dot_general x0 -> x4, matrix products: none -> 5.9 us  [the longest x1 2.2 us: on_device(): jnp.dot(placing, own_rows, preferred_element_type=f32).astype(bf16)]
  transfers between devices with their start and end apart: 9 -> 7, of which waited for: 6 -> 4; matrix products, arithmetic and copies ran while one was open for 15% -> 10% of each run, Pallas kernels for 0% -> 0%
where the time goes in v1:
time: 365 us; the launch traced here: 364 us
  waiting for transfers between devices  145 us (40%)
  blocking collectives  137 us (38%)
  matrix products  49.9 us (14%)
  between operations  14.1 us (4%)
  other arithmetic  12.5 us (3%)
  starting transfers between devices  5.21 us (1%)
    reduce_scatter x1, waiting for transfers between devices, on_device(): lax.psum_scatter(expert_term, 'tp', scatter_dimension=2, tiled=True)  58 us
    all_to_all x1, blocking collectives, on_device(): lax.all_to_all(sent_rows, 'sp', split_axis=0, concat_axis=0, tiled=True)  44.2 us
    reduce_scatter x1, waiting for transfers between devices, on_device(): lax.psum_scatter(jnp.einsum('td,tc->dc', grad_resid, merged, preferred_el...  42.8 us
    all_to_all x1, blocking collectives, on_device(): lax.all_to_all(summed, 'sp', split_axis=0, concat_axis=0, tiled=True)  42.4 us
    all_to_all x1, blocking collectives, on_device(): lax.all_to_all(sent_cots, 'sp', split_axis=0, concat_axis=0, tiled=True)  40.2 us
    all_gather x1, waiting for transfers between devices, on_device(): lax.all_gather(lax.all_to_all(sent_cots, 'sp', split_axis=0, concat_axis=...  30.3 us
    all_gather x1, waiting for transfers between devices, on_device(): lax.all_gather(own_grad.astype(bf16), 'tp', axis=1, tiled=True).astype(f32)  14.1 us
    all_to_all x1, blocking collectives, on_device(): lax.all_to_all(sent_weights, 'sp', split_axis=0, concat_axis=0, tiled=True)  9.85 us
  transfers between devices with their start and end apart: 7, of which 4 were waited for; matrix products, arithmetic and copies ran while one was open for 10% of the time, Pallas kernels for 0%

profile of v1, /device:TPU:0, one launch (start us, length us, event | category | flops | bytes accessed | tf_op | source)
XLA Modules:
  0.0 364.5 jit_solution(5835447940842580865)
XLA Ops:
  7.3 3.6 convert_element_type.75
  10.8 0.4 multiply_reduce_fusion.1
  11.6 2.2 convolution_convert_fusion.1
  13.8 44.2 %all_to_all.24 = bf16[8,192,512]{2,1,0:T(8,128)(2,1)} all-to-all(bf16[8,192,512]{2,1,0:T(8,128)(2,1)S(1)} %bitcast.47), channel_id=1, replica_groups=mesh['sp'=8,'tp'=4] {'sp'}, dimensions={0} | all-to-all | bytes 3145728 | tf_op jit(solution)/shard_map/all_to_all | solution.py:95
  58.1 2.0 convolution_convert_fusion
  60.1 40.2 %all_to_all.25 = bf16[8,192,512]{2,1,0:T(8,128)(2,1)} all-to-all(bf16[8,192,512]{2,1,0:T(8,128)(2,1)S(1)} %bitcast.48), channel_id=1, replica_groups=mesh['sp'=8,'tp'=4] {'sp'}, dimensions={0} | all-to-all | bytes 3145728 | tf_op jit(solution)/shard_map/all_to_all | solution.py:99
  100.4 0.6 add_reduce_fusion
  101.0 9.9 %all_to_all.26 = f32[8,1,192]{2,1,0:T(1,128)S(1)} all-to-all(f32[8,1,192]{2,1,0:T(1,128)S(1)} %all_to_all.17), channel_id=1, replica_groups=mesh['sp'=8,'tp'=4] {'sp'}, dimensions={0} | all-to-all | bytes 12288 | tf_op jit(solution)/shard_map/all_to_all | solution.py:93
  111.0 6.7 %fusion.17 = f32[1536,256]{1,0:T(8,128)} fusion(bf16[1536,2048]{1,0:T(8,128)(2,1)} %bitcast.55, bf16[1,2048,256]{2,1,0:T(8,128)(2,1)S(1)} %copy-done), kind=kOutput, calls=%fused_computation.32 | convolution fusion | flops 1610612736 | bytes 8912896 | tf_op jit(solution)/shard_map/dot_general | solution.py:18
  117.7 0.5 copy-done.17
  118.2 3.0 fusion.20
  121.2 30.3 %all-gather.6.cloned.1.call-done = bf16[8,192,2048]{2,1,0:T(8,128)(2,1)} async-done(((bf16[8,192,512]{2,1,0:T(8,128)(2,1)}), bf16[8,192,2048]{2,1,0:T(8,128)(2,1)}) %all-gather.6.cloned.1.call-update) | async-done | bytes 6291472 | tf_op jit(solution)/shard_map/all_gather | solution.py:98
  151.5 6.4 %multiply_convert_fusion.1 = (bf16[1536,256]{1,0:T(8,128)(2,1)S(1)}, bf16[1536,256]{1,0:T(8,128)(2,1)S(1)}) fusion(f32[1536,256]{1,0:T(8,128)} %fusion.17, f32[1536,256]{1,0:T(8,128)} %fusion.20, f32[1536]{0:T(1024)S(1)} %mul.171, bf16[1536,2048]{1,0:T(8,128)(2,1)} %bitcast.59, bf16[1,256,2048]{2,1,0:T(8,128)(2,1)} %param.20), kind=kOutput, calls=%fused_computation.17 | convolution fusion | flops 1616117760 | bytes 12064768 | tf_op jit(solution)/shard_map/rd,fd->rf/dot_general | solution.py:25
  158.0 1.8 fusion.15
  159.8 4.4 %add_convert_fusion = bf16[1536,2048]{1,0:T(8,128)(2,1)} fusion(f32[1536,2048]{1,0:T(8,128)S(1)} %fusion.15, bf16[1536,256]{1,0:T(8,128)(2,1)S(1)} %get-tuple-element.16, bf16[1,2048,256]{2,1,0:T(8,128)(2,1)S(1)} %copy-done.6), kind=kOutput, calls=%fused_computation | convolution fusion | flops 1616904192 | bytes 20709376 | tf_op jit(solution)/shard_map/rf,df->rd/dot_general | solution.py:32
  164.3 58.0 %reduce-scatter.3.cloned.1.call-done = bf16[8,192,512]{2,1,0:T(8,128)(2,1)} async-done(((bf16[8,192,2048]{2,1,0:T(8,128)(2,1)}), bf16[8,192,512]{2,1,0:T(8,128)(2,1)}) %reduce-scatter.3.cloned.1.call-update) | async-done | bytes 1572880 | tf_op jit(solution)/shard_map/reduce_scatter | solution.py:115
  222.3 42.4 %all_to_all.27 = bf16[8,192,512]{2,1,0:T(8,128)(2,1)S(1)} all-to-all(bf16[8,192,512]{2,1,0:T(8,128)(2,1)} %reduce-scatter.3.cloned.1.call-done), channel_id=1, replica_groups=mesh['sp'=8,'tp'=4] {'sp'}, dimensions={0} | all-to-all | bytes 3145728 | tf_op jit(solution)/shard_map/all_to_all | solution.py:119
  264.7 1.6 fusion.6
  266.4 3.6 collective-permute-start
  270.0 14.1 %all-gather.8.cloned.1.call-done = bf16[384,2048]{1,0:T(8,128)(2,1)} async-done(((bf16[384,512]{1,0:T(8,128)(2,1)}), bf16[384,2048]{1,0:T(8,128)(2,1)}) %all-gather.8.cloned.1.call-update) | async-done | bytes 1572880 | tf_op jit(solution)/shard_map/all_gather | solution.py:123
  284.1 2.1 multiply_reduce_fusion
  286.3 2.5 subtract_convert_fusion
  288.9 1.3 multiply_convert_fusion.4
  290.2 1.8 convolution_convert_fusion.2
  292.0 6.2 %convolution_bitcast_fusion.2 = f32[1,2048,256]{2,1,0:T(8,128)} fusion(bf16[1536,2048]{1,0:T(8,128)(2,1)} %bitcast.56, bf16[1536,256]{1,0:T(8,128)(2,1)S(1)} %get-tuple-element.17), kind=kOutput, calls=%fused_computation.10 | convolution fusion | flops 1610612736 | bytes 9175040 | tf_op jit(solution)/shard_map/rd,rf->df/dot_general | solution.py:30
  298.2 6.3 %convolution_bitcast_fusion = f32[1,256,2048]{2,1,0:T(8,128)} fusion(bf16[1536,2048]{1,0:T(8,128)(2,1)} %bitcast.60, f32[1536,256]{1,0:T(8,128)S(1)} %copy-done.21, f32[1536]{0:T(1024)S(1)} %mul.171, f32[1536,256]{1,0:T(8,128)S(1)} %copy-done.20), kind=kOutput, calls=%fused_computation.8 | convolution fusion | flops 1613365248 | bytes 11540480 | tf_op jit(solution)/shard_map/rf,rd->fd/dot_general | solution.py:23
  304.5 1.4 collective-permute-start.1
  305.9 6.1 %convolution_bitcast_fusion.1 = f32[1,2048,256]{2,1,0:T(8,128)} fusion(bf16[1536,2048]{1,0:T(8,128)(2,1)} %bitcast.57, bf16[1536,256]{1,0:T(8,128)(2,1)S(1)} %copy-done.8), kind=kOutput, calls=%fused_computation.9 | convolution fusion | flops 1610612736 | bytes 9175040 | tf_op jit(solution)/shard_map/rd,rf->df/dot_general | solution.py:31
  312.0 0.8 fusion.35
  312.9 0.7 fusion.36
  313.6 42.8 %reduce-scatter.5.cloned.1.call-done = bf16[256,256]{1,0:T(8,128)(2,1)} async-done(((bf16[2048,256]{1,0:T(8,128)(2,1)}), bf16[256,256]{1,0:T(8,128)(2,1)}) %reduce-scatter.5.cloned.1.call-update) | async-done | bytes 131088 | tf_op jit(solution)/shard_map/reduce_scatter | solution.py:138
  356.3 1.6 convert_element_type.92
  (72 shorter events, 1.0 us)
Async XLA Ops:
  7.2 103.8 %copy-start = (bf16[1,2048,256]{2,1,0:T(8,128)(2,1)S(1)}, bf16[1,2048,256]{2,1,0:T(8,128)(2,1)}, u32[]{:S(2)}) copy-start(bf16[1,2048,256]{2,1,0:T(8,128)(2,1)} %param.18) | copy-start | bytes 3145732
  7.2 103.8 %all-gather.4.cloned.1.call-start = ((), (), s32[]{:S(2)}) async-start(), calls=%async_computation.6 | async-start | bytes 7864320 | tf_op jit(solution)/shard_map/all_gather | solution.py:94
  7.2 3.6 copy-start.2
  7.2 4.0 %copy-start.14 = (s32[384,2]{0,1:T(2,128)S(1)}, s32[384,2]{0,1:T(2,128)}, u32[]{:S(2)}) copy-start(s32[384,2]{0,1:T(2,128)} %param.16) | copy-start | bytes 9220
  7.3 4.3 %copy-start.13 = (f32[2048]{0:T(1024)S(1)}, f32[2048]{0:T(1024)}, u32[]{:S(2)}) copy-start(f32[2048]{0:T(1024)} %param.15) | copy-start | bytes 24580
  58.0 93.5 %all-gather.6.cloned.1.call-start = ((), (), s32[]{:S(2)}) async-start(), calls=%async_computation.7 | async-start | bytes 7864320 | tf_op jit(solution)/shard_map/all_gather | solution.py:98
  60.1 40.3 %copy-start.15 = (f32[384,2]{0,1:T(2,128)S(1)}, f32[384,2]{0,1:T(2,128)}, u32[]{:S(2)}) copy-start(f32[384,2]{0,1:T(2,128)} %param.17) | copy-start | bytes 9220
  100.3 122.0 %reduce-scatter.3.cloned.1.call-start = ((), (), s32[]{:S(2)}) async-start(), calls=%async_computation.8 | async-start | bytes 7864320 | tf_op jit(solution)/shard_map/reduce_scatter | solution.py:115
  111.0 6.7 %copy-start.5 = (bf16[1,2048,256]{2,1,0:T(8,128)(2,1)S(1)}, bf16[1,2048,256]{2,1,0:T(8,128)(2,1)}, u32[]{:S(2)}) copy-start(bf16[1,2048,256]{2,1,0:T(8,128)(2,1)} %param.19) | copy-start | bytes 3145732
  111.0 7.2 %copy-start.17 = (bf16[8,192,2048]{2,1,0:T(8,128)(2,1)S(1)}, bf16[8,192,2048]{2,1,0:T(8,128)(2,1)}, u32[]{:S(2)}) copy-start(bf16[8,192,2048]{2,1,0:T(8,128)(2,1)} %all-gather.4.cloned.1.call-done) | copy-start | bytes 18874372
  158.0 1.9 copy-start.7
  158.0 1.9 copy-start.6
  164.3 119.9 %all-gather.8.cloned.1.call-start = ((), (), s32[]{:S(2)}) async-start(), calls=%async_computation.9 | async-start | bytes 1966080 | tf_op jit(solution)/shard_map/all_gather | solution.py:123
  264.7 1.7 copy-start.9
  264.7 1.7 copy-start.11
  264.7 5.3 %copy-start.16 = (f32[3,256]{1,0:T(4,128)S(1)}, f32[3,256]{1,0:T(4,128)}, u32[]{:S(2)}) copy-start(f32[3,256]{1,0:T(4,128)} %param.25) | copy-start | bytes 9220
  266.3 90.0 %reduce-scatter.5.cloned.1.call-start = ((), (), s32[]{:S(2)}) async-start(), calls=%async_computation.10 | async-start | bytes 1179648 | tf_op jit(solution)/shard_map/reduce_scatter | solution.py:138
  266.4 22.4 %collective-permute-start = (f32[2,256]{1,0:T(2,128)S(1)}, f32[2,256]{1,0:T(2,128)S(1)}, u32[]{:S(2)}, u32[]{:S(2)}) collective-permute-start(f32[2,256]{1,0:T(2,128)S(1)} %slice.57), channel_id=1, source_target_pairs={{0,4},{4,8},{8,12},{12,16},{16,20},{20,24},{24,28},{1,5},{5,9},{9,... | collective-permute-start | bytes 6152 | tf_op jit(solution)/shard_map/ppermute | solution.py:12
  284.1 2.1 copy-start.3
  286.3 2.6 copy-start.18
  286.3 2.6 copy-start.19
  288.8 1.3 copy-start.4
  292.0 6.2 %copy-start.20 = (f32[1536,256]{1,0:T(8,128)S(1)}, f32[1536,256]{1,0:T(8,128)}, u32[]{:S(2)}) copy-start(f32[1536,256]{1,0:T(8,128)} %fusion.17) | copy-start | bytes 4718596
  292.0 6.2 %copy-start.21 = (f32[1536,256]{1,0:T(8,128)S(1)}, f32[1536,256]{1,0:T(8,128)}, u32[]{:S(2)}) copy-start(f32[1536,256]{1,0:T(8,128)} %fusion.20) | copy-start | bytes 4718596
  298.2 7.7 %copy-start.8 = (bf16[1536,256]{1,0:T(8,128)(2,1)S(1)}, bf16[1536,256]{1,0:T(8,128)(2,1)}, u32[]{:S(2)}) copy-start(bf16[1536,256]{1,0:T(8,128)(2,1)} %copy-done.7) | copy-start | bytes 2359300
  304.5 7.6 %copy-start.12 = (bf16[384,256]{1,0:T(8,128)(2,1)S(1)}, bf16[384,256]{1,0:T(8,128)(2,1)}, u32[]{:S(2)}) copy-start(bf16[384,256]{1,0:T(8,128)(2,1)} %param.23) | copy-start | bytes 589828
  304.5 8.4 %copy-start.10 = (bf16[384,256]{1,0:T(8,128)(2,1)S(1)}, bf16[384,256]{1,0:T(8,128)(2,1)}, u32[]{:S(2)}) copy-start(bf16[384,256]{1,0:T(8,128)(2,1)} %param.24) | copy-start | bytes 589828
  304.5 7.6 %collective-permute-start.1 = (f32[2,256]{1,0:T(2,128)S(1)}, f32[2,256]{1,0:T(2,128)S(1)}, u32[]{:S(2)}, u32[]{:S(2)}) collective-permute-start(f32[2,256]{1,0:T(2,128)S(1)} %slice.60), channel_id=1, source_target_pairs={{4,0},{8,4},{12,8},{16,12},{20,16},{24,20},{28,24},{5,1},{9,5},{13... | collective-permute-start | bytes 6152 | tf_op jit(solution)/shard_map/ppermute | solution.py:12
  305.9 52.1 %copy-start.1 = (bf16[1,2048,256]{2,1,0:T(8,128)(2,1)S(1)}, bf16[1,2048,256]{2,1,0:T(8,128)(2,1)}, u32[]{:S(2)}) copy-start(bf16[1,2048,256]{2,1,0:T(8,128)(2,1)} %param.18) | copy-start | bytes 3145732
Sparse Core Ops, SparseCore 0:
  58.2 45.3 all-gather.3
  105.1 46.3 all-gather.5
  164.4 57.8 reduce-scatter.2
  266.4 17.6 all-gather.7
  292.1 64.1 reduce-scatter.4

commit v2 on v1

--- a/solution.py
+++ b/solution.py
@@ -1,6 +1,10 @@
+import functools
+
 import jax
 import jax.numpy as jnp
 from jax import lax
+from jax.experimental import pallas as pl
+from jax.experimental.pallas import tpu as pltpu
 from jax.sharding import PartitionSpec as P
 
 norm_eps = 1e-06
@@ -10,6 +14,321 @@
     size = lax.axis_size(axis)
     pairs = [(i, i + by) for i in range(size) if 0 <= i + by < size]
     return lax.ppermute(array, axis, pairs)
+
+
+def remote(source, target, send_sem, recv_sem, **device):
+    return pltpu.make_async_remote_copy(
+        src_ref=source,
+        dst_ref=target,
+        send_sem=send_sem,
+        recv_sem=recv_sem,
+        device_id=device,
+        device_id_type=pl.DeviceIdType.MESH,
+    )
+
+
+def greet(groups, spot, core_peer, far_peer):
+    barrier = pltpu.get_barrier_semaphore()
+
+    def to_group(offset, carry):
+        pl.semaphore_signal(
+            barrier,
+            inc=1,
+            device_id={"sp": lax.rem(spot + offset, groups)},
+            device_id_type=pl.DeviceIdType.MESH,
+        )
+        return carry
+
+    lax.fori_loop(1, groups, to_group, 0)
+    for peer in (core_peer, far_peer):
+        pl.semaphore_signal(
+            barrier, inc=1, device_id={"tp": peer}, device_id_type=pl.DeviceIdType.MESH
+        )
+    pl.semaphore_wait(barrier, groups + 1)
+
+
+def dispatch_kernel(
+    groups,
+    lanes,
+    sent_rows,
+    sent_cots,
+    sent_weights,
+    got_rows,
+    got_cots,
+    got_weights,
+    local_sem,
+    send_a,
+    recv_a,
+    send_x,
+    recv_x,
+    send_c,
+    recv_c,
+    send_f,
+    recv_f,
+    send_w,
+    recv_w,
+):
+    spot, lane = lax.axis_index("sp"), lax.axis_index("tp")
+    core_peer = lane + 1 - 2 * lax.rem(lane, 2)
+    far_peer = lax.rem(lane + lanes // 2, lanes)
+    quarter = sent_rows.shape[2]
+    pairs = ((sent_rows, got_rows), (sent_cots, got_cots))
+
+    def part(ref, block, who):
+        return ref.at[block, :, pl.ds(pl.multiple_of(who * quarter, quarter), quarter)]
+
+    def across(k, offset):
+        goal = lax.rem(spot + offset, groups)
+        return remote(
+            pairs[k][0].at[goal],
+            part(pairs[k][1], spot, lane),
+            send_a.at[k, offset],
+            recv_a.at[k, offset],
+            sp=goal,
+        )
+
+    def weights_across(offset):
+        goal = lax.rem(spot + offset, groups)
+        return remote(
+            sent_weights.at[goal],
+            got_weights.at[spot],
+            send_w.at[offset],
+            recv_w.at[offset],
+            sp=goal,
+        )
+
+    def origin(offset):
+        return lax.rem(spot - offset + groups, groups)
+
+    def sideways(k, offset, source, far):
+        sems = (send_x, recv_x) if far else (send_c, recv_c)
+        return remote(
+            source,
+            part(pairs[k][1], origin(offset), lane),
+            sems[0].at[k, offset],
+            sems[1].at[k, offset],
+            tp=far_peer if far else core_peer,
+        )
+
+    def forward(k, offset):
+        held = part(pairs[k][1], origin(offset), far_peer)
+        return remote(held, held, send_f.at[k, offset], recv_f.at[k, offset], tp=core_peer)
+
+    greet(groups, spot, core_peer, far_peer)
+    own = [
+        pltpu.make_async_copy(
+            pairs[k][0].at[spot], part(pairs[k][1], spot, lane), local_sem.at[k]
+        )
+        for k in (0, 1)
+    ]
+    own_weights = pltpu.make_async_copy(
+        sent_weights.at[spot], got_weights.at[spot], local_sem.at[2]
+    )
+
+    def launch(offset, carry):
+        weights_across(offset).start()
+        for k in (0, 1):
+            across(k, offset).start()
+        return carry
+
+    lax.fori_loop(1, groups, launch, 0)
+    for k in (0, 1):
+        for far in (True, False):
+            sideways(k, 0, pairs[k][0].at[spot], far).start()
+    for copy in own:
+        copy.start()
+    own_weights.start()
+
+    def pass_on(offset, carry):
+        for k in (0, 1):
+            across(k, offset).wait_recv()
+            for far in (True, False):
+                sideways(k, offset, part(pairs[k][1], origin(offset), lane), far).start()
+        for k in (0, 1):
+            sideways(k, offset - 1, part(pairs[k][1], origin(offset - 1), lane), True).wait_recv()
+            forward(k, offset - 1).start()
+        return carry
+
+    lax.fori_loop(1, groups, pass_on, 0)
+    for k in (0, 1):
+        last = groups - 1
+        sideways(k, last, part(pairs[k][1], origin(last), lane), True).wait_recv()
+        forward(k, last).start()
+
+    def finish(offset, carry):
+        for k in (0, 1):
+            mine = part(pairs[k][1], origin(offset), lane)
+            sideways(k, offset, mine, True).wait_send()
+            sideways(k, offset, mine, False).wait()
+            forward(k, offset).wait()
+        return carry
+
+    def finish_across(offset, carry):
+        weights_across(offset).wait()
+        for k in (0, 1):
+            across(k, offset).wait_send()
+        return carry
+
+    lax.fori_loop(0, groups, finish, 0)
+    lax.fori_loop(1, groups, finish_across, 0)
+    for copy in own:
+        copy.wait()
+    own_weights.wait()
+
+
+def dispatch(sent_rows, sent_cots, sent_weights, groups, lanes):
+    span, quarter = sent_rows.shape[1:]
+    whole = jax.ShapeDtypeStruct((groups, span, quarter * lanes), sent_rows.dtype)
+    sem = pltpu.SemaphoreType.DMA
+    anywhere = pl.BlockSpec(memory_space=pl.ANY)
+    wire = 2 * span * quarter * 2 * groups * 3
+    return pl.pallas_call(
+        functools.partial(dispatch_kernel, groups, lanes),
+        out_shape=(
+            whole,
+            whole,
+            jax.ShapeDtypeStruct(sent_weights.shape, sent_weights.dtype),
+        ),
+        in_specs=[anywhere] * 3,
+        out_specs=(anywhere,) * 3,
+        scratch_shapes=[sem((3,))] + [sem((2, groups))] * 8 + [sem((groups,))] * 2,
+        compiler_params=pltpu.CompilerParams(collective_id=1, has_side_effects=True),
+        cost_estimate=pl.CostEstimate(
+            flops=0, bytes_accessed=40 * wire, transcendentals=0
+        ),
+        name="dispatch",
+    )(sent_rows, sent_cots, sent_weights)
+
+
+def collect_kernel(
+    groups,
+    lanes,
+    partial,
+    returned,
+    from_core,
+    to_far,
+    from_far,
+    summed,
+    send_c,
+    recv_c,
+    send_x,
+    recv_x,
+    send_a,
+    recv_a,
+):
+    f32 = jnp.float32
+    bf16 = jnp.bfloat16
+    spot, lane = lax.axis_index("sp"), lax.axis_index("tp")
+    core_peer = lane + 1 - 2 * lax.rem(lane, 2)
+    far_peer = lax.rem(lane + lanes // 2, lanes)
+    quarter = returned.shape[2]
+
+    def part(block, who):
+        return partial.at[block, :, pl.ds(pl.multiple_of(who * quarter, quarter), quarter)]
+
+    def goal_of(step):
+        return lax.rem(spot + step + 1, groups)
+
+    def to_core(step, far):
+        who = lax.rem(core_peer + far * (lanes // 2), lanes)
+        return remote(
+            part(goal_of(step), who),
+            from_core.at[step, far],
+            send_c.at[step, far],
+            recv_c.at[step, far],
+            tp=core_peer,
+        )
+
+    def to_far_peer(step):
+        return remote(
+            to_far.at[step], from_far.at[step], send_x.at[step], recv_x.at[step], tp=far_peer
+        )
+
+    def home(step):
+        goal = goal_of(step)
+        return remote(
+            summed.at[step], returned.at[spot], send_a.at[step], recv_a.at[step], sp=goal
+        )
+
+    greet(groups, spot, core_peer, far_peer)
+
+    def begin(step, carry):
+        to_core(step, 1).start()
+        to_core(step, 0).start()
+        return carry
+
+    lax.fori_loop(0, groups, begin, 0)
+
+    def middle(step, carry):
+        to_core(step, 1).wait_recv()
+        to_far[step] = (
+            part(goal_of(step), far_peer)[...].astype(f32) + from_core[step, 1].astype(f32)
+        ).astype(bf16)
+        to_far_peer(step).start()
+        return carry
+
+    lax.fori_loop(0, groups, middle, 0)
+
+    def total(step):
+        to_core(step, 0).wait_recv()
+        to_far_peer(step).wait_recv()
+        return (
+            part(goal_of(step), lane)[...].astype(f32)
+            + from_core[step, 0].astype(f32)
+            + from_far[step].astype(f32)
+        ).astype(bf16)
+
+    def end(step, carry):
+        summed[step] = total(step)
+        home(step).start()
+        return carry
+
+    lax.fori_loop(0, groups - 1, end, 0)
+    returned[spot] = total(groups - 1)
+
+    def finish(step, carry):
+        to_core(step, 0).wait_send()
+        to_core(step, 1).wait_send()
+        to_far_peer(step).wait_send()
+        return carry
+
+    lax.fori_loop(0, groups, finish, 0)
+
+    def finish_home(step, carry):
+        home(step).wait()
+        return carry
+
+    lax.fori_loop(0, groups - 1, finish_home, 0)
+
+
+def collect(partial, groups, lanes):
+    span, width = partial.shape[1:]
+    quarter = width // lanes
+    block = (groups, span, quarter)
+    sem = pltpu.SemaphoreType.DMA
+    inside = pl.BlockSpec(memory_space=pltpu.VMEM)
+    return pl.pallas_call(
+        functools.partial(collect_kernel, groups, lanes),
+        out_shape=jax.ShapeDtypeStruct(block, partial.dtype),
+        in_specs=[inside],
+        out_specs=inside,
+        scratch_shapes=[
+            pltpu.VMEM((groups, 2, span, quarter), partial.dtype),
+            pltpu.VMEM(block, partial.dtype),
+            pltpu.VMEM(block, partial.dtype),
+            pltpu.VMEM(block, partial.dtype),
+            sem((groups, 2)),
+            sem((groups, 2)),
+        ]
+        + [sem((groups,))] * 4,
+        compiler_params=pltpu.CompilerParams(
+            collective_id=2, has_side_effects=True, vmem_limit_bytes=40 * 2**20
+        ),
+        cost_estimate=pl.CostEstimate(
+            flops=0, bytes_accessed=150 * 2**20, transcendentals=0
+        ),
+        name="collect",
+    )(partial)
 
 
 def expert_pass(entry_rows, entry_cots, entry_weights, gate_mat, up_mat, down_mat):
@@ -90,15 +409,12 @@
     sent_cots = jnp.dot(placing, own_cots, preferred_element_type=f32).astype(bf16)
     sent_rows = sent_rows.reshape(groups, slot_span, quarter)
     sent_cots = sent_cots.reshape(groups, slot_span, quarter)
-    got_weights = lax.all_to_all(sent_weights, "sp", split_axis=0, concat_axis=0, tiled=True)
-    got_rows = lax.all_gather(
-        lax.all_to_all(sent_rows, "sp", split_axis=0, concat_axis=0, tiled=True),
-        "tp", axis=2, tiled=True,
-    )
-    got_cots = lax.all_gather(
-        lax.all_to_all(sent_cots, "sp", split_axis=0, concat_axis=0, tiled=True),
-        "tp", axis=2, tiled=True,
-    )
+    padded = -(-slot_span // 128) * 128
+    sent_weights = jnp.broadcast_to(
+        jnp.pad(sent_weights, ((0, 0), (0, padded - slot_span)))[:, None, :], (groups, 8, padded)
+    )
+    got_rows, got_cots, got_weights = dispatch(sent_rows, sent_cots, sent_weights, groups, lanes)
+    got_weights = got_weights[:, 0, :slot_span]
     grads_gate, grads_up, grads_down, terms = ([], [], [], [])
     entry_rows = got_rows.reshape(groups * capacity, model_width)
     entry_cots = got_cots.reshape(groups * capacity, model_width)
@@ -111,14 +427,7 @@
     grads_down.append(grad_down)
     terms.append(partial_sum.astype(bf16).reshape(groups, capacity, model_width))
     expert_term = terms[0]
-    summed = (
-        lax.psum_scatter(expert_term, "tp", scatter_dimension=2, tiled=True)
-        .astype(jnp.float32)
-        .astype(bf16)
-    )
-    returned = lax.all_to_all(summed, "sp", split_axis=0, concat_axis=0, tiled=True).reshape(
-        expert_total * capacity, model_width // lanes
-    )
+    returned = collect(expert_term, groups, lanes).reshape(slots, quarter)
     own_grad = jnp.einsum("st,sq->tq", placing, returned, preferred_element_type=f32)
     dnormed = lax.all_gather(own_grad.astype(bf16), "tp", axis=1, tiled=True).astype(f32)
     scaled = dnormed * norm_gain

time: 365 us -> 303 us (0.83)
  Pallas kernels: 0 us -> 157 us
  blocking collectives: 137 us -> 0 us
  waiting for transfers between devices: 145 us -> 57.2 us
    pallas_call x0 -> x2, Pallas kernels: none -> 157 us  [the longest x1 93.4 us: dispatch(): pl.pallas_call(functools.partial(dispatch_kernel, groups, lanes), out_sha...]
    all_to_all x4 -> x0, blocking collectives: 137 us -> none  [the longest x1 44.2 us: on_device(): lax.all_to_all(sent_rows, 'sp', split_axis=0, concat_axis=0, tiled=True)]
    reduce_scatter x1 -> x0, waiting for transfers between devices: 58 us -> none  [on_device(): lax.psum_scatter(expert_term, 'tp', scatter_dimension=2, tiled=True)]
    all_gather x2 -> x0, waiting for transfers between devices: 30.3 us -> none  [the longest x1 30.3 us: on_device(): lax.all_gather(lax.all_to_all(sent_cots, 'sp', split_axis=0, concat_axis=...]
  transfers between devices with their start and end apart: 7 -> 4, of which waited for: 4 -> 2; matrix products, arithmetic and copies ran while one was open for 10% -> 8% of each run, Pallas kernels for 0% -> 0%
where the time goes in v2:
time: 303 us
  Pallas kernels  157 us (52%)
  waiting for transfers between devices  57.2 us (19%)
  matrix products  50.9 us (17%)
  between operations  14.3 us (5%)
  other arithmetic  12.1 us (4%)
  starting transfers between devices  8.29 us (3%)
  local copies, waits for them, and re-layouts  3.09 us (1%)
    pallas_call x1, Pallas kernels, dispatch(): pl.pallas_call(functools.partial(dispatch_kernel, groups, lanes), out_sha...  93.4 us
    pallas_call x1, Pallas kernels, collect(): pl.pallas_call(functools.partial(collect_kernel, groups, lanes), out_shap...  63.4 us
    reduce_scatter x1, waiting for transfers between devices, on_device(): lax.psum_scatter(jnp.einsum('td,tc->dc', grad_resid, merged, preferred_el...  42.8 us
    all_gather x1, waiting for transfers between devices, on_device(): lax.all_gather(own_grad.astype(bf16), 'tp', axis=1, tiled=True).astype(f32)  14.3 us
    ppermute x2, starting transfers between devices, passed_along(): return lax.ppermute(array, axis, pairs)  8.21 us
    dot_general x1, matrix products, expert_pass(): jnp.einsum('rd,fd->rf', entry_cots, down_mat, preferred_element_type=f32)  6.97 us
    dot_general x1, matrix products, expert_pass(): jnp.einsum('rf,rd->fd', hidden, entry_cots, preferred_element_type=f32)  6.26 us
    dot_general x1, matrix products, expert_pass(): jnp.einsum('rd,rf->df', entry_rows, dgate, preferred_element_type=f32)  6.15 us
  transfers between devices with their start and end apart: 4, of which 2 were waited for; matrix products, arithmetic and copies ran while one was open for 8% of the time, Pallas kernels for 0%

profile of v2, /device:TPU:0, one launch (start us, length us, event | category | flops | bytes accessed | tf_op | source)
XLA Modules:
  0.0 302.7 jit_solution(2228844328435363692)
XLA Ops:
  7.3 3.6 %convert_element_type.75 = f32[384,2048]{1,0:T(8,128)} convert(bf16[384,2048]{1,0:T(8,128)(2,1)} %param.13) | non-fusion elementwise | flops 786432 | bytes 4718592 | tf_op jit(solution)/shard_map/convert_element_type | solution.py:381
  10.9 0.4 multiply_reduce_fusion.1
  11.7 3.1 %convolution_convert_fusion = bf16[1536,512]{1,0:T(8,128)(2,1)} fusion(s32[384]{0:T(512)S(1)} %get-tuple-element.17, s32[384]{0:T(512)S(1)} %get-tuple-element.16, bf16[384,2048]{1,0:T(8,128)(2,1)} %param.14, s32[]{:T(128)S(6)} %select_n.16), kind=kOutput, calls=%fused_computation.5 | convolution fusion | flops 606535680 | bytes 1969156 | tf_op jit(solution)/shard_map/dot_general | solution.py:409
  14.8 0.6 add_reduce_fusion
  15.4 3.4 %convolution_convert_fusion.1 = bf16[1536,512]{1,0:T(8,128)(2,1)} fusion(s32[384]{0:T(512)S(1)} %get-tuple-element.17, s32[384]{0:T(512)S(1)} %get-tuple-element.16, f32[384,2048]{1,0:T(8,128)} %convert_element_type.75, s32[]{:T(128)S(6)} %select_n.16, f32[512]{0:T(512)S(1)} %dynamic-slice, f32[384]{0:T(512)S(1)} %get-tuple-element.29), kind=kOutput, calls=%fused_computation.6 | convolution fusion | flops 607125504 | bytes 2365956 | tf_op jit(solution)/shard_map/dot_general | solution.py:408
  18.8 0.6 broadcast_in_dim.57.sent_weights
  19.4 93.4 %dispatch.1 = (bf16[8,192,2048]{2,1,0:T(8,128)(2,1)}, bf16[8,192,2048]{2,1,0:T(8,128)(2,1)}, f32[8,8,256]{2,1,0:T(8,128)}) custom-call(bf16[8,192,512]{2,1,0:T(8,128)(2,1)} %bitcast.48, bf16[8,192,512]{2,1,0:T(8,128)(2,1)} %bitcast.47, f32[8,8,256]{2,1,0:T(8,128)} %broadcast_in_dim.57.sent_weights), custom_call_target="tpu_custom_call" | custom-call | bytes 377487360 | tf_op jit(solution)/shard_map/dispatch/pallas_call | solution.py:185
  112.9 5.9 %fusion.17 = f32[1536,256]{1,0:T(8,128)} fusion(bf16[1536,2048]{1,0:T(8,128)(2,1)} %bitcast.55, bf16[1,2048,256]{2,1,0:T(8,128)(2,1)S(1)} %copy-done), kind=kOutput, calls=%fused_computation.32 | convolution fusion | flops 1610612736 | bytes 8912896 | tf_op jit(solution)/shard_map/dot_general | solution.py:337
  118.8 3.0 fusion.20
  121.8 0.9 slice_reduce_fusion
  122.7 7.0 %multiply_convert_fusion.1 = (bf16[1536,256]{1,0:T(8,128)(2,1)}, bf16[1536,256]{1,0:T(8,128)(2,1)S(1)}) fusion(f32[1536,256]{1,0:T(8,128)} %fusion.17, f32[1536,256]{1,0:T(8,128)} %fusion.20, f32[1536]{0:T(1024)S(1)} %mul.171, bf16[1536,2048]{1,0:T(8,128)(2,1)} %bitcast.59, bf16[1,256,2048]{2,1,0:T(8,128)(2,1)S(1)} %copy-done.17), kind=kOutput, calls=%fused_computation.17 | convolution fusion | flops 1616117760 | bytes 12064768 | tf_op jit(solution)/shard_map/rd,fd->rf/dot_general | solution.py:344
  129.7 1.8 fusion.15
  131.5 3.5 %add_convert_fusion = bf16[1536,2048]{1,0:T(8,128)(2,1)S(1)} fusion(f32[1536,2048]{1,0:T(8,128)S(1)} %fusion.15, bf16[1536,256]{1,0:T(8,128)(2,1)} %get-tuple-element.22, bf16[1,2048,256]{2,1,0:T(8,128)(2,1)} %param.19), kind=kOutput, calls=%fused_computation | convolution fusion | flops 1616904192 | bytes 20709376 | tf_op jit(solution)/shard_map/rf,df->rd/dot_general | solution.py:351
  135.0 63.4 %collect.1 = bf16[8,192,512]{2,1,0:T(8,128)(2,1)S(1)} custom-call(bf16[8,192,2048]{2,1,0:T(8,128)(2,1)S(1)} %bitcast.45), custom_call_target="tpu_custom_call" | custom-call | bytes 157286400 | tf_op jit(solution)/shard_map/collect/pallas_call | solution.py:310
  198.4 1.6 fusion.6
  200.0 1.1 convert_multiply_fusion.2
  201.1 0.7 copy-done.10
  201.9 6.8 %collective-permute-start = (f32[2,256]{1,0:T(2,128)S(1)}, f32[2,256]{1,0:T(2,128)S(1)}, u32[]{:S(2)}, u32[]{:S(2)}) collective-permute-start(f32[2,256]{1,0:T(2,128)S(1)} %slice.61), channel_id=1, source_target_pairs={{0,4},{4,8},{8,12},{12,16},{16,20},{20,24},{24,28},{1,5},{5,9},{9,... | collective-permute-start | bytes 6152 | tf_op jit(solution)/shard_map/ppermute | solution.py:16
  208.7 14.3 %all-gather.2.cloned.1.call-done = bf16[384,2048]{1,0:T(8,128)(2,1)} async-done(((bf16[384,512]{1,0:T(8,128)(2,1)}), bf16[384,2048]{1,0:T(8,128)(2,1)}) %all-gather.2.cloned.1.call-update) | async-done | bytes 1572880 | tf_op jit(solution)/shard_map/all_gather | solution.py:432
  223.0 2.1 multiply_reduce_fusion
  225.4 1.0 subtract_convert_fusion
  226.5 0.3 copy-done.18
  226.8 1.3 multiply_convert_fusion.4
  228.1 1.8 convolution_convert_fusion.2
  229.9 6.2 %convolution_bitcast_fusion.2 = f32[1,2048,256]{2,1,0:T(8,128)} fusion(bf16[1536,2048]{1,0:T(8,128)(2,1)} %bitcast.56, bf16[1536,256]{1,0:T(8,128)(2,1)S(1)} %get-tuple-element.23), kind=kOutput, calls=%fused_computation.10 | convolution fusion | flops 1610612736 | bytes 9175040 | tf_op jit(solution)/shard_map/rd,rf->df/dot_general | solution.py:349
  236.1 6.3 %convolution_bitcast_fusion = f32[1,256,2048]{2,1,0:T(8,128)} fusion(bf16[1536,2048]{1,0:T(8,128)(2,1)} %bitcast.60, f32[1536,256]{1,0:T(8,128)S(1)} %copy-done.21, f32[1536]{0:T(1024)S(1)} %mul.171, f32[1536,256]{1,0:T(8,128)S(1)} %copy-done.20), kind=kOutput, calls=%fused_computation.8 | convolution fusion | flops 1613365248 | bytes 11540480 | tf_op jit(solution)/shard_map/rf,rd->fd/dot_general | solution.py:342
  242.3 1.4 collective-permute-start.1
  243.7 6.0 %convolution_bitcast_fusion.1 = f32[1,2048,256]{2,1,0:T(8,128)} fusion(bf16[1536,2048]{1,0:T(8,128)(2,1)} %bitcast.57, bf16[1536,256]{1,0:T(8,128)(2,1)S(1)} %copy-done.7), kind=kOutput, calls=%fused_computation.9 | convolution fusion | flops 1610612736 | bytes 9175040 | tf_op jit(solution)/shard_map/rd,rf->df/dot_general | solution.py:350
  249.8 0.8 fusion.35
  250.6 0.7 fusion.36
  251.4 42.8 %reduce-scatter.2.cloned.1.call-done = bf16[256,256]{1,0:T(8,128)(2,1)} async-done(((bf16[2048,256]{1,0:T(8,128)(2,1)}), bf16[256,256]{1,0:T(8,128)(2,1)}) %reduce-scatter.2.cloned.1.call-update) | async-done | bytes 131088 | tf_op jit(solution)/shard_map/reduce_scatter | solution.py:447
  294.2 1.6 convert_element_type.92
  (63 shorter events, 0.9 us)
Async XLA Ops:
  7.2 105.7 %copy-start = (bf16[1,2048,256]{2,1,0:T(8,128)(2,1)S(1)}, bf16[1,2048,256]{2,1,0:T(8,128)(2,1)}, u32[]{:S(2)}) copy-start(bf16[1,2048,256]{2,1,0:T(8,128)(2,1)} %param.18) | copy-start | bytes 3145732
  7.2 215.9 %all-gather.2.cloned.1.call-start = ((), (), s32[]{:S(2)}) async-start(), calls=%async_computation.1 | async-start | bytes 1966080 | tf_op jit(solution)/shard_map/all_gather | solution.py:432
  7.2 3.6 %copy-start.1 = (bf16[384,2048]{1,0:T(8,128)(2,1)S(1)}, bf16[384,2048]{1,0:T(8,128)(2,1)}, u32[]{:S(2)}) copy-start(bf16[384,2048]{1,0:T(8,128)(2,1)} %param.13) | copy-start | bytes 4718596
  7.2 4.0 %copy-start.13 = (s32[384,2]{0,1:T(2,128)S(1)}, s32[384,2]{0,1:T(2,128)}, u32[]{:S(2)}) copy-start(s32[384,2]{0,1:T(2,128)} %param.16) | copy-start | bytes 9220
  7.3 4.3 %copy-start.14 = (f32[384,2]{0,1:T(2,128)S(1)}, f32[384,2]{0,1:T(2,128)}, u32[]{:S(2)}) copy-start(f32[384,2]{0,1:T(2,128)} %param.17) | copy-start | bytes 9220
  7.3 4.3 %copy-start.12 = (f32[2048]{0:T(1024)S(1)}, f32[2048]{0:T(1024)}, u32[]{:S(2)}) copy-start(f32[2048]{0:T(1024)} %param.15) | copy-start | bytes 24580
  112.8 5.9 %copy-start.6 = (bf16[1,2048,256]{2,1,0:T(8,128)(2,1)S(1)}, bf16[1,2048,256]{2,1,0:T(8,128)(2,1)}, u32[]{:S(2)}) copy-start(bf16[1,2048,256]{2,1,0:T(8,128)(2,1)} %param.19) | copy-start | bytes 3145732
  112.9 5.9 %copy-start.16 = (bf16[8,192,2048]{2,1,0:T(8,128)(2,1)S(1)}, bf16[8,192,2048]{2,1,0:T(8,128)(2,1)}, u32[]{:S(2)}) copy-start(bf16[8,192,2048]{2,1,0:T(8,128)(2,1)} %get-tuple-element.11) | copy-start | bytes 18874372
  118.8 4.0 %copy-start.17 = (bf16[1,256,2048]{2,1,0:T(8,128)(2,1)S(1)}, bf16[1,256,2048]{2,1,0:T(8,128)(2,1)}, u32[]{:S(2)}) copy-start(bf16[1,256,2048]{2,1,0:T(8,128)(2,1)} %param.20) | copy-start | bytes 3145732
  198.4 10.3 %copy-start.15 = (f32[3,256]{1,0:T(4,128)S(1)}, f32[3,256]{1,0:T(4,128)}, u32[]{:S(2)}) copy-start(f32[3,256]{1,0:T(4,128)} %param.25) | copy-start | bytes 9220
  198.4 24.7 %copy-start.2 = (bf16[384,2048]{1,0:T(8,128)(2,1)S(1)}, bf16[384,2048]{1,0:T(8,128)(2,1)}, u32[]{:S(2)}) copy-start(bf16[384,2048]{1,0:T(8,128)(2,1)} %param.13) | copy-start | bytes 4718596
  200.0 94.2 %reduce-scatter.2.cloned.1.call-start = ((), (), s32[]{:S(2)}) async-start(), calls=%async_computation.2 | async-start | bytes 1179648 | tf_op jit(solution)/shard_map/reduce_scatter | solution.py:447
  201.1 0.7 copy-start.10
  201.9 24.6 %collective-permute-start = (f32[2,256]{1,0:T(2,128)S(1)}, f32[2,256]{1,0:T(2,128)S(1)}, u32[]{:S(2)}, u32[]{:S(2)}) collective-permute-start(f32[2,256]{1,0:T(2,128)S(1)} %slice.61), channel_id=1, source_target_pairs={{0,4},{4,8},{8,12},{12,16},{16,20},{20,24},{24,28},{1,5},{5,9},{9,... | collective-permute-start | bytes 6152 | tf_op jit(solution)/shard_map/ppermute | solution.py:16
  223.0 2.2 copy-start.3
  223.0 2.4 copy-start.4
  225.4 1.1 copy-start.11
  225.4 1.3 copy-start.18
  225.4 1.4 copy-start.19
  226.4 1.6 copy-start.5
  229.9 6.2 %copy-start.20 = (f32[1536,256]{1,0:T(8,128)S(1)}, f32[1536,256]{1,0:T(8,128)}, u32[]{:S(2)}) copy-start(f32[1536,256]{1,0:T(8,128)} %fusion.17) | copy-start | bytes 4718596
  229.9 6.2 %copy-start.21 = (f32[1536,256]{1,0:T(8,128)S(1)}, f32[1536,256]{1,0:T(8,128)}, u32[]{:S(2)}) copy-start(f32[1536,256]{1,0:T(8,128)} %fusion.20) | copy-start | bytes 4718596
  236.1 7.7 %copy-start.7 = (bf16[1536,256]{1,0:T(8,128)(2,1)S(1)}, bf16[1536,256]{1,0:T(8,128)(2,1)}, u32[]{:S(2)}) copy-start(bf16[1536,256]{1,0:T(8,128)(2,1)} %get-tuple-element.22) | copy-start | bytes 2359300
  242.3 7.5 %copy-start.9 = (bf16[384,256]{1,0:T(8,128)(2,1)S(1)}, bf16[384,256]{1,0:T(8,128)(2,1)}, u32[]{:S(2)}) copy-start(bf16[384,256]{1,0:T(8,128)(2,1)} %param.23) | copy-start | bytes 589828
  242.3 8.3 %copy-start.8 = (bf16[384,256]{1,0:T(8,128)(2,1)S(1)}, bf16[384,256]{1,0:T(8,128)(2,1)}, u32[]{:S(2)}) copy-start(bf16[384,256]{1,0:T(8,128)(2,1)} %param.24) | copy-start | bytes 589828
  242.3 7.5 %collective-permute-start.1 = (f32[2,256]{1,0:T(2,128)S(1)}, f32[2,256]{1,0:T(2,128)S(1)}, u32[]{:S(2)}, u32[]{:S(2)}) collective-permute-start(f32[2,256]{1,0:T(2,128)S(1)} %slice.64), channel_id=1, source_target_pairs={{4,0},{8,4},{12,8},{16,12},{20,16},{24,20},{28,24},{5,1},{9,5},{13... | collective-permute-start | bytes 6152 | tf_op jit(solution)/shard_map/ppermute | solution.py:16
Sparse Core Ops, SparseCore 0:
  200.1 22.8 all-gather.1
  230.0 64.1 reduce-scatter.1

commit v3 on v2

--- a/solution.py
+++ b/solution.py
@@ -328,6 +328,104 @@
             flops=0, bytes_accessed=150 * 2**20, transcendentals=0
         ),
         name="collect",
+    )(partial)
+
+
+def gather_kernel(groups, lanes, mine, gathered, own_sem, send_sems, recv_sems):
+    spot, lane = lax.axis_index("sp"), lax.axis_index("tp")
+    core_peer = lane + 1 - 2 * lax.rem(lane, 2)
+    far_peer = lax.rem(lane + lanes // 2, lanes)
+    quarter = mine.shape[1]
+
+    def part(who):
+        return gathered.at[:, pl.ds(pl.multiple_of(who * quarter, quarter), quarter)]
+
+    greet(groups, spot, core_peer, far_peer)
+    far = remote(mine, part(lane), send_sems.at[0], recv_sems.at[0], tp=far_peer)
+    near = remote(mine, part(lane), send_sems.at[1], recv_sems.at[1], tp=core_peer)
+    own = pltpu.make_async_copy(mine, part(lane), own_sem)
+    far.start()
+    near.start()
+    own.start()
+    far.wait_recv()
+    passed = remote(
+        part(far_peer), part(far_peer), send_sems.at[2], recv_sems.at[2], tp=core_peer
+    )
+    passed.start()
+    far.wait_send()
+    near.wait()
+    own.wait()
+    passed.wait()
+
+
+def gather_quarters(mine, groups, lanes):
+    sem = pltpu.SemaphoreType.DMA
+    inside = pl.BlockSpec(memory_space=pltpu.VMEM)
+    return pl.pallas_call(
+        functools.partial(gather_kernel, groups, lanes),
+        out_shape=jax.ShapeDtypeStruct((mine.shape[0], mine.shape[1] * lanes), mine.dtype),
+        in_specs=[inside],
+        out_specs=inside,
+        scratch_shapes=[sem, sem((3,)), sem((3,))],
+        compiler_params=pltpu.CompilerParams(collective_id=3, has_side_effects=True),
+        name="gather_quarters",
+    )(mine)
+
+
+def reduce_kernel(groups, lanes, partial, total, arrived, send_sems, recv_sems):
+    f32 = jnp.float32
+    spot, lane = lax.axis_index("sp"), lax.axis_index("tp")
+    core_peer = lane + 1 - 2 * lax.rem(lane, 2)
+    far_peer = lax.rem(lane + lanes // 2, lanes)
+
+    def across(offset):
+        goal = lax.rem(spot + offset, groups)
+        return remote(
+            partial.at[goal],
+            arrived.at[offset],
+            send_sems.at[offset],
+            recv_sems.at[offset],
+            sp=goal,
+        )
+
+    greet(groups, spot, core_peer, far_peer)
+
+    def launch(offset, carry):
+        across(offset).start()
+        return carry
+
+    lax.fori_loop(1, groups, launch, 0)
+    total[...] = partial[spot].astype(f32)
+
+    def add(offset, carry):
+        across(offset).wait_recv()
+        total[...] += arrived[offset].astype(f32)
+        return carry
+
+    lax.fori_loop(1, groups, add, 0)
+
+    def finish(offset, carry):
+        across(offset).wait_send()
+        return carry
+
+    lax.fori_loop(1, groups, finish, 0)
+
+
+def reduce_rows(partial, groups, lanes):
+    sem = pltpu.SemaphoreType.DMA
+    inside = pl.BlockSpec(memory_space=pltpu.VMEM)
+    return pl.pallas_call(
+        functools.partial(reduce_kernel, groups, lanes),
+        out_shape=jax.ShapeDtypeStruct(partial.shape[1:], jnp.float32),
+        in_specs=[inside],
+        out_specs=inside,
+        scratch_shapes=[
+            pltpu.VMEM(partial.shape, partial.dtype),
+            sem((groups,)),
+            sem((groups,)),
+        ],
+        compiler_params=pltpu.CompilerParams(collective_id=4, has_side_effects=True),
+        name="reduce_rows",
     )(partial)
 
 
@@ -429,7 +527,7 @@
     expert_term = terms[0]
     returned = collect(expert_term, groups, lanes).reshape(slots, quarter)
     own_grad = jnp.einsum("st,sq->tq", placing, returned, preferred_element_type=f32)
-    dnormed = lax.all_gather(own_grad.astype(bf16), "tp", axis=1, tiled=True).astype(f32)
+    dnormed = gather_quarters(own_grad.astype(bf16), groups, lanes).astype(f32)
     scaled = dnormed * norm_gain
     resid_grad = (
         cotangent.astype(f32)
@@ -444,14 +542,12 @@
         + taps[2] * extended[2 : token_count + 2]
     )
     merged = (gate_b.astype(f32) * conv).astype(bf16)
-    grad_out_weight = lax.psum_scatter(
-        jnp.einsum("td,tc->dc", grad_resid, merged, preferred_element_type=f32).astype(
-            jnp.bfloat16
-        ),
-        "sp",
-        scatter_dimension=0,
-        tiled=True,
-    ).astype(jnp.float32)
+    out_partial = jnp.einsum("td,tc->dc", grad_resid, merged, preferred_element_type=f32)
+    grad_out_weight = reduce_rows(
+        out_partial.astype(bf16).reshape(groups, model_width // groups, merged.shape[1]),
+        groups,
+        lanes,
+    )
     dmerged = jnp.dot(grad_resid, out_weight, preferred_element_type=f32)
     grad_gate_b = (dmerged * conv).astype(bf16)
     dconv = dmerged * gate_b.astype(f32)

time: 303 us -> 270 us (0.89); the launches traced: 303 us -> 265 us
  waiting for transfers between devices: 57.2 us -> 0.01 us
  Pallas kernels: 157 us -> 199 us
  between operations: 14.3 us -> 1.03 us
  matrix products: 50.9 us -> 44.3 us
    pallas_call x0 -> x2, Pallas kernels: none -> 43.2 us  [the longest x1 23.3 us: reduce_rows(): pl.pallas_call(functools.partial(reduce_kernel, groups, lanes), out_shape...]
    reduce_scatter x1 -> x0, waiting for transfers between devices: 42.8 us -> none  [on_device(): lax.psum_scatter(jnp.einsum('td,tc->dc', grad_resid, merged, preferred_el...]
    all_gather x1 -> x0, waiting for transfers between devices: 14.3 us -> none  [on_device(): lax.all_gather(own_grad.astype(bf16), 'tp', axis=1, tiled=True).astype(f32)]
  transfers between devices with their start and end apart: 4 -> 2, of which waited for: 2 -> 0; matrix products, arithmetic and copies ran while one was open for 8% -> 20% of each run, Pallas kernels for 0% -> 75%
where the time goes in v3:
time: 270 us; the launch traced here: 265 us
  Pallas kernels  199 us (74%)
  matrix products  44.3 us (16%)
  other arithmetic  10.5 us (4%)
  starting transfers between devices  6.31 us (2%)
  local copies, waits for them, and re-layouts  3.98 us (1%)
    pallas_call x1, Pallas kernels, dispatch(): pl.pallas_call(functools.partial(dispatch_kernel, groups, lanes), out_sha...  92.2 us
    pallas_call x1, Pallas kernels, collect(): pl.pallas_call(functools.partial(collect_kernel, groups, lanes), out_shap...  63.3 us
    pallas_call x1, Pallas kernels, reduce_rows(): pl.pallas_call(functools.partial(reduce_kernel, groups, lanes), out_shape...  23.3 us
    pallas_call x1, Pallas kernels, gather_quarters(): pl.pallas_call(functools.partial(gather_kernel, groups, lanes), out_shape...  19.8 us
    dot_general x1, matrix products, expert_pass(): jnp.einsum('rf,rd->fd', hidden, entry_cots, preferred_element_type=f32)  7.12 us
    ppermute x2, starting transfers between devices, passed_along(): return lax.ppermute(array, axis, pairs)  6.31 us
    dot_general x1, matrix products, expert_pass(): gate_pre = jnp.dot(entry_rows, gate_mat, preferred_element_type=f32)  5.88 us
    dot_general x1, matrix products, expert_pass(): jnp.einsum('rd,fd->rf', entry_cots, down_mat, preferred_element_type=f32)  5.44 us
  transfers between devices with their start and end apart: 2, of which 0 were waited for; matrix products, arithmetic and copies ran while one was open for 20% of the time, Pallas kernels for 75%

profile of v3, /device:TPU:0, one launch (start us, length us, event | category | flops | bytes accessed | tf_op | source)
XLA Modules:
  0.0 264.8 jit_solution(17670718595064728071)
XLA Ops:
  0.6 1.2 convert_multiply_fusion.2
  1.8 4.9 %collective-permute-start = (f32[2,256]{1,0:T(2,128)S(1)}, f32[2,256]{1,0:T(2,128)S(1)}, u32[]{:S(2)}, u32[]{:S(2)}) collective-permute-start(f32[2,256]{1,0:T(2,128)S(1)} %slice.61), channel_id=1, source_target_pairs={{0,4},{4,8},{8,12},{12,16},{16,20},{20,24},{24,28},{1,5},{5,9},{9,... | collective-permute-start | bytes 6152 | tf_op jit(solution)/shard_map/ppermute | solution.py:16
  6.8 3.5 %convert_element_type.72 = f32[384,2048]{1,0:T(8,128)} convert(bf16[384,2048]{1,0:T(8,128)(2,1)} %param.13) | non-fusion elementwise | flops 786432 | bytes 4718592 | tf_op jit(solution)/shard_map/convert_element_type | solution.py:479
  10.3 0.4 multiply_reduce_fusion.1
  11.1 3.1 %convolution_convert_fusion = bf16[1536,512]{1,0:T(8,128)(2,1)} fusion(s32[384]{0:T(512)S(1)} %get-tuple-element.17, s32[384]{0:T(512)S(1)} %get-tuple-element.16, bf16[384,2048]{1,0:T(8,128)(2,1)} %param.14, s32[]{:T(128)S(6)} %select_n.16), kind=kOutput, calls=%fused_computation.5 | convolution fusion | flops 606535680 | bytes 1969156 | tf_op jit(solution)/shard_map/dot_general | solution.py:507
  14.3 0.6 add_reduce_fusion
  14.9 3.3 %convolution_convert_fusion.1 = bf16[1536,512]{1,0:T(8,128)(2,1)} fusion(s32[384]{0:T(512)S(1)} %get-tuple-element.17, s32[384]{0:T(512)S(1)} %get-tuple-element.16, f32[384,2048]{1,0:T(8,128)} %convert_element_type.72, s32[]{:T(128)S(6)} %select_n.16, f32[512]{0:T(512)S(1)} %dynamic-slice, f32[384]{0:T(512)S(1)} %get-tuple-element.29), kind=kOutput, calls=%fused_computation.6 | convolution fusion | flops 607125504 | bytes 2365956 | tf_op jit(solution)/shard_map/dot_general | solution.py:506
  18.2 0.6 broadcast_in_dim.57.sent_weights
  18.9 92.2 %dispatch.1 = (bf16[8,192,2048]{2,1,0:T(8,128)(2,1)}, bf16[8,192,2048]{2,1,0:T(8,128)(2,1)}, f32[8,8,256]{2,1,0:T(8,128)}) custom-call(bf16[8,192,512]{2,1,0:T(8,128)(2,1)} %bitcast.49, bf16[8,192,512]{2,1,0:T(8,128)(2,1)} %bitcast.48, f32[8,8,256]{2,1,0:T(8,128)} %broadcast_in_dim.57.sent_weights), custom_call_target="tpu_custom_call" | custom-call | bytes 377487360 | tf_op jit(solution)/shard_map/dispatch/pallas_call | solution.py:185
  111.1 5.9 %fusion.17 = f32[1536,256]{1,0:T(8,128)} fusion(bf16[1536,2048]{1,0:T(8,128)(2,1)} %bitcast.57, bf16[1,2048,256]{2,1,0:T(8,128)(2,1)S(1)} %copy-done), kind=kOutput, calls=%fused_computation.32 | convolution fusion | flops 1610612736 | bytes 8912896 | tf_op jit(solution)/shard_map/dot_general | solution.py:435
  117.0 3.0 %fusion.20 = f32[1536,256]{1,0:T(8,128)} fusion(bf16[1536,2048]{1,0:T(8,128)(2,1)S(1)} %bitcast.58, bf16[1,2048,256]{2,1,0:T(8,128)(2,1)S(1)} %copy-done.6), kind=kOutput, calls=%fused_computation.35 | convolution fusion | flops 1610612736 | bytes 8912896 | tf_op jit(solution)/shard_map/dot_general | solution.py:436
  120.0 0.9 slice_reduce_fusion
  120.9 7.1 %convolution_bitcast_fusion = f32[1,256,2048]{2,1,0:T(8,128)} fusion(bf16[1536,2048]{1,0:T(8,128)(2,1)} %bitcast.63, f32[1536,256]{1,0:T(8,128)} %fusion.20, f32[1536]{0:T(1024)S(1)} %mul.171, f32[1536,256]{1,0:T(8,128)} %fusion.17), kind=kOutput, calls=%fused_computation.8 | convolution fusion | flops 1613365248 | bytes 11540480 | tf_op jit(solution)/shard_map/rf,rd->fd/dot_general | solution.py:440
  128.1 5.4 %multiply_convert_fusion.1 = (bf16[1536,256]{1,0:T(8,128)(2,1)S(1)}, bf16[1536,256]{1,0:T(8,128)(2,1)S(1)}) fusion(f32[1536,256]{1,0:T(8,128)S(1)} %copy-done.20, f32[1536,256]{1,0:T(8,128)S(1)} %copy-done.21, f32[1536]{0:T(1024)S(1)} %mul.171, bf16[1536,2048]{1,0:T(8,128)(2,1)} %bitcast.64, bf16[1,256,2048]{2,1,0:T(8,128)(2,1)S(1)} %copy-done.17), kind=kOutput, calls=%fused_computation.17 | convolution fusion | flops 1616117760 | bytes 12064768 | tf_op jit(solution)/shard_map/rd,fd->rf/dot_general | solution.py:442
  133.5 3.2 %convolution_bitcast_fusion.2 = f32[1,2048,256]{2,1,0:T(8,128)} fusion(bf16[1536,2048]{1,0:T(8,128)(2,1)S(1)} %bitcast.61, bf16[1536,256]{1,0:T(8,128)(2,1)S(1)} %get-tuple-element.23), kind=kOutput, calls=%fused_computation.10 | convolution fusion | flops 1610612736 | bytes 9175040 | tf_op jit(solution)/shard_map/rd,rf->df/dot_general | solution.py:447
  136.8 1.8 fusion.15
  138.6 3.5 %convolution_bitcast_fusion.1 = f32[1,2048,256]{2,1,0:T(8,128)} fusion(bf16[1536,2048]{1,0:T(8,128)(2,1)S(1)} %bitcast.62, bf16[1536,256]{1,0:T(8,128)(2,1)S(1)} %get-tuple-element.22), kind=kOutput, calls=%fused_computation.9 | convolution fusion | flops 1610612736 | bytes 9175040 | tf_op jit(solution)/shard_map/rd,rf->df/dot_general | solution.py:448
  142.1 3.1 %add_convert_fusion = bf16[1536,2048]{1,0:T(8,128)(2,1)S(1)} fusion(f32[1536,2048]{1,0:T(8,128)S(1)} %fusion.15, bf16[1536,256]{1,0:T(8,128)(2,1)} %copy-done.7, bf16[1,2048,256]{2,1,0:T(8,128)(2,1)S(1)} %copy-done.6), kind=kOutput, calls=%fused_computation | convolution fusion | flops 1616904192 | bytes 20709376 | tf_op jit(solution)/shard_map/rf,df->rd/dot_general | solution.py:449
  145.2 63.3 %collect.1 = bf16[8,192,512]{2,1,0:T(8,128)(2,1)S(1)} custom-call(bf16[8,192,2048]{2,1,0:T(8,128)(2,1)S(1)} %bitcast.46), custom_call_target="tpu_custom_call" | custom-call | bytes 157286400 | tf_op jit(solution)/shard_map/collect/pallas_call | solution.py:310
  208.6 1.6 fusion.6.mine
  210.1 19.8 %gather_quarters.1 = bf16[384,2048]{1,0:T(8,128)(2,1)} custom-call(bf16[384,512]{1,0:T(8,128)(2,1)} %fusion.6.mine), custom_call_target="tpu_custom_call" | custom-call | tf_op jit(solution)/shard_map/gather_quarters/pallas_call | solution.py:364
  230.0 2.2 multiply_reduce_fusion
  232.2 0.2 copy-done.4
  232.4 1.1 subtract_convert_fusion
  233.5 0.2 copy-done.18
  233.7 1.3 multiply_convert_fusion.4
  235.0 1.4 collective-permute-start.1
  236.4 1.7 convolution_convert_fusion.2
  238.2 23.3 %reduce_rows.1 = f32[256,256]{1,0:T(8,128)} custom-call(bf16[8,256,256]{2,1,0:T(8,128)(2,1)} %bitcast.50), custom_call_target="tpu_custom_call" | custom-call | tf_op jit(solution)/shard_map/reduce_rows/pallas_call | solution.py:417
  261.5 0.8 fusion.35
  262.4 0.7 fusion.36
  263.1 1.7 copy.24
  (64 shorter events, 0.7 us)
Async XLA Ops:
  0.6 110.4 %copy-start = (bf16[1,2048,256]{2,1,0:T(8,128)(2,1)S(1)}, bf16[1,2048,256]{2,1,0:T(8,128)(2,1)}, u32[]{:S(2)}) copy-start(bf16[1,2048,256]{2,1,0:T(8,128)(2,1)} %param.18) | copy-start | bytes 3145732
  1.8 4.9 %copy-start.10 = (f32[384,256]{1,0:T(8,128)}, f32[384,256]{1,0:T(8,128)S(1)}, u32[]{:S(2)}) copy-start(f32[384,256]{1,0:T(8,128)S(1)} %convert_multiply_fusion.2) | copy-start | bytes 1179652
  1.8 231.6 %collective-permute-start = (f32[2,256]{1,0:T(2,128)S(1)}, f32[2,256]{1,0:T(2,128)S(1)}, u32[]{:S(2)}, u32[]{:S(2)}) collective-permute-start(f32[2,256]{1,0:T(2,128)S(1)} %slice.61), channel_id=1, source_target_pairs={{0,4},{4,8},{8,12},{12,16},{16,20},{20,24},{24,28},{1,5},{5,9},{9,... | collective-permute-start | bytes 6152 | tf_op jit(solution)/shard_map/ppermute | solution.py:16
  6.7 3.6 %copy-start.1 = (bf16[384,2048]{1,0:T(8,128)(2,1)S(1)}, bf16[384,2048]{1,0:T(8,128)(2,1)}, u32[]{:S(2)}) copy-start(bf16[384,2048]{1,0:T(8,128)(2,1)} %param.13) | copy-start | bytes 4718596
  6.8 4.0 %copy-start.13 = (s32[384,2]{0,1:T(2,128)S(1)}, s32[384,2]{0,1:T(2,128)}, u32[]{:S(2)}) copy-start(s32[384,2]{0,1:T(2,128)} %param.16) | copy-start | bytes 9220
  6.8 4.2 %copy-start.14 = (f32[384,2]{0,1:T(2,128)S(1)}, f32[384,2]{0,1:T(2,128)}, u32[]{:S(2)}) copy-start(f32[384,2]{0,1:T(2,128)} %param.17) | copy-start | bytes 9220
  6.8 4.3 %copy-start.12 = (f32[2048]{0:T(1024)S(1)}, f32[2048]{0:T(1024)}, u32[]{:S(2)}) copy-start(f32[2048]{0:T(1024)} %param.15) | copy-start | bytes 24580
  111.1 5.9 %copy-start.6 = (bf16[1,2048,256]{2,1,0:T(8,128)(2,1)S(1)}, bf16[1,2048,256]{2,1,0:T(8,128)(2,1)}, u32[]{:S(2)}) copy-start(bf16[1,2048,256]{2,1,0:T(8,128)(2,1)} %param.19) | copy-start | bytes 3145732
  111.1 5.9 %copy-start.16 = (bf16[8,192,2048]{2,1,0:T(8,128)(2,1)S(1)}, bf16[8,192,2048]{2,1,0:T(8,128)(2,1)}, u32[]{:S(2)}) copy-start(bf16[8,192,2048]{2,1,0:T(8,128)(2,1)} %get-tuple-element.11) | copy-start | bytes 18874372
  120.9 7.1 %copy-start.17 = (bf16[1,256,2048]{2,1,0:T(8,128)(2,1)S(1)}, bf16[1,256,2048]{2,1,0:T(8,128)(2,1)}, u32[]{:S(2)}) copy-start(bf16[1,256,2048]{2,1,0:T(8,128)(2,1)} %param.20) | copy-start | bytes 3145732
  120.9 7.1 %copy-start.20 = (f32[1536,256]{1,0:T(8,128)S(1)}, f32[1536,256]{1,0:T(8,128)}, u32[]{:S(2)}) copy-start(f32[1536,256]{1,0:T(8,128)} %fusion.17) | copy-start | bytes 4718596
  120.9 7.1 %copy-start.21 = (f32[1536,256]{1,0:T(8,128)S(1)}, f32[1536,256]{1,0:T(8,128)}, u32[]{:S(2)}) copy-start(f32[1536,256]{1,0:T(8,128)} %fusion.20) | copy-start | bytes 4718596
  120.9 12.6 %slice-start = ((s8[6291456]{0:T(1024)(128)(4,1)}), s8[4194304]{0:T(1024)(128)(4,1)S(1)}, s32[]{:S(2)}) async-start(s8[6291456]{0:T(1024)(128)(4,1)} %bitcast.59), calls=%async_computation | async-start | bytes 8388608
  128.1 5.5 %slice-start.1 = ((s8[6291456]{0:T(1024)(128)(4,1)}), s8[2097152]{0:T(1024)(128)(4,1)S(1)}, s32[]{:S(2)}) async-start(s8[6291456]{0:T(1024)(128)(4,1)} %bitcast.59), calls=%async_computation.1 | async-start | bytes 4194304
  133.5 5.1 %copy-start.7 = (bf16[1536,256]{1,0:T(8,128)(2,1)}, bf16[1536,256]{1,0:T(8,128)(2,1)S(1)}, u32[]{:S(2)}) copy-start(bf16[1536,256]{1,0:T(8,128)(2,1)S(1)} %get-tuple-element.22) | copy-start | bytes 2359300
  210.1 19.8 %copy-start.2 = (bf16[384,2048]{1,0:T(8,128)(2,1)S(1)}, bf16[384,2048]{1,0:T(8,128)(2,1)}, u32[]{:S(2)}) copy-start(bf16[384,2048]{1,0:T(8,128)(2,1)} %param.13) | copy-start | bytes 4718596
  230.0 2.2 copy-start.3
  230.0 2.3 copy-start.4
  232.3 1.1 copy-start.15
  232.4 1.1 copy-start.11
  232.4 1.4 copy-start.18
  232.4 1.4 copy-start.19
  233.4 4.7 %copy-start.5 = (bf16[384,2048]{1,0:T(8,128)(2,1)}, bf16[384,2048]{1,0:T(8,128)(2,1)S(1)}, u32[]{:S(2)}) copy-start(bf16[384,2048]{1,0:T(8,128)(2,1)S(1)} %subtract_convert_fusion) | copy-start | bytes 4718596
  235.0 26.5 %copy-start.9 = (bf16[384,256]{1,0:T(8,128)(2,1)S(1)}, bf16[384,256]{1,0:T(8,128)(2,1)}, u32[]{:S(2)}) copy-start(bf16[384,256]{1,0:T(8,128)(2,1)} %param.23) | copy-start | bytes 589828
  235.0 26.5 %collective-permute-start.1 = (f32[2,256]{1,0:T(2,128)S(1)}, f32[2,256]{1,0:T(2,128)S(1)}, u32[]{:S(2)}, u32[]{:S(2)}) collective-permute-start(f32[2,256]{1,0:T(2,128)S(1)} %slice.64), channel_id=1, source_target_pairs={{4,0},{8,4},{12,8},{16,12},{20,16},{24,20},{28,24},{5,1},{9,5},{13... | collective-permute-start | bytes 6152 | tf_op jit(solution)/shard_map/ppermute | solution.py:16
  236.4 26.0 %copy-start.8 = (bf16[384,256]{1,0:T(8,128)(2,1)S(1)}, bf16[384,256]{1,0:T(8,128)(2,1)}, u32[]{:S(2)}) copy-start(bf16[384,256]{1,0:T(8,128)(2,1)} %param.24) | copy-start | bytes 589828
